TPU v7x, 128 devices: a whole 4x4x4 slice. The times are simulated.
128 devices in a mesh: sp: 16 (over z, y), tp: 8 (over x, core).
Axes of the slice: x: 4, y: 4, z: 4, core: 2. Of those that a mesh axis runs over, the one named last changes fastest.
Arguments:
- query_first: bfloat16 [12288, 8, 128], P('sp', 'tp'), may hold values from -5.375 to 5.375
- key_first: bfloat16 [12288, 8, 128], P('sp', 'tp'), may hold values from -5.375 to 5.375
- value_first: bfloat16 [12288, 8, 128], P('sp', 'tp'), may hold values from -6 to 6
- query_second: bfloat16 [12288, 8, 256], P('sp', 'tp'), may hold values from -5.375 to 5.375
- key_second: bfloat16 [12288, 8, 256], P('sp', 'tp'), may hold values from -5.375 to 5.375
- value_second: bfloat16 [12288, 8, 128], P('sp', 'tp'), may hold values from -6 to 6
- mix_lambda: float32 [2, 8], P(None, 'tp'), may hold values from 0.3 to 0.8
- head_gain: float32 [2, 8, 128], P(None, 'tp'), may hold values from 0.1 to 1.9
- out_weight: bfloat16 [2, 8, 128, 2048], P(None, 'tp'), may hold values from -0.125 to 0.125
- residual: bfloat16 [12288, 2048], P(('sp', 'tp')), may hold values from -6 to 6
- norm_gain: float32 [2, 2048], replicated, may hold values from 0.1 to 1.9
- up_weight: bfloat16 [2048, 8192], P('sp', 'tp'), may hold values from -0.125 to 0.125
- down_weight: bfloat16 [8192, 2048], P('tp', 'sp'), may hold values from -0.0625 to 0.0625
Outputs:
- mixed: bfloat16 [12288, 2048], P(('sp', 'tp'))
All inputs are finite; a program needn't handle non-finite values.
Results may differ from a plain program's by a relative error of at most 0.02.
Values may be sent and summed in bfloat16 or wider, within the bound.
A program may use at most 128 MiB of HBM per device.

v0:
```python
import math

import jax
import jax.numpy as jnp
from jax import lax
from jax.sharding import PartitionSpec as P

EPSILON = 1e-05
LOWEST = -1e30


def rows_first(arrays, axis, dims):
    turned = [jnp.moveaxis(a, dim, 0) for a, dim in zip(arrays, dims)]
    both = jnp.concatenate([t.reshape(len(t), -1) for t in turned], axis=1)
    out, at, gathered = (lax.all_gather(both, axis, axis=0, tiled=True), 0, [])
    for t, dim in zip(turned, dims):
        share = out[:, at : at + t[0].size].reshape(-1, *t.shape[1:])
        gathered.append(jnp.moveaxis(share, 0, dim))
        at += t[0].size
    return tuple(gathered)


def side_by_side(arrays, axis, dim, along):
    both = jnp.concatenate(arrays, axis=along)
    out, at, gathered = (lax.all_gather(both, axis, axis=dim, tiled=True), 0, [])
    for a in arrays:
        gathered.append(lax.slice_in_dim(out, at, at + a.shape[along], axis=along))
        at += a.shape[along]
    return tuple(gathered)


def in_blocks(shard, dim, count):
    shape = shard.shape
    parts = shard.reshape(*shape[:dim], count, shape[dim] // count, *shape[dim + 1 :])
    return jnp.moveaxis(parts, dim, 0)


def sum_at_owner(shard, axis, dim):
    parts = in_blocks(shard, dim, lax.axis_size(axis))
    arrived = lax.all_to_all(parts, axis, split_axis=0, concat_axis=0, tiled=True)
    return arrived.astype(jnp.float32).sum(axis=0)


def layer_norm(activations, scales):
    average = jnp.mean(activations, axis=-1, keepdims=True)
    centred = activations - average
    spread = jnp.mean(centred * centred, axis=-1, keepdims=True)
    return centred * lax.rsqrt(spread + EPSILON) * scales


def fold_group(carried, queries, key_rows, values, score_scale):
    maxima, totals, numerator = carried
    scores = (
        jnp.einsum("qhck,phck->hcqp", queries, key_rows, preferred_element_type=jnp.float32)
        * score_scale
    )
    newest = jnp.maximum(maxima, jnp.max(scores, axis=-1))
    weights = jnp.exp(scores - newest[..., None])
    factor = jnp.exp(maxima - newest)
    totals = totals * factor + jnp.sum(weights, axis=-1)
    numerator = numerator * factor[..., None] + jnp.einsum(
        "hcqp,phv->hcqv", weights.astype(jnp.bfloat16), values, preferred_element_type=jnp.float32
    )
    return (newest, totals, numerator)


def finish_group(carried, lambdas, gains):
    maxima, totals, numerator = carried
    attended = (
        numerator[:, 0] / totals[:, 0, :, None]
        - lambdas[:, None, None] * numerator[:, 1] / totals[:, 1, :, None]
    )
    mean_square = jnp.mean(attended * attended, axis=-1, keepdims=True)
    return (attended * lax.rsqrt(mean_square + EPSILON) * gains[:, None, :]).astype(jnp.bfloat16)


def squared_relu(expanded):
    return jnp.square(jnp.maximum(expanded, 0.0)).astype(jnp.bfloat16)


def local(
    query_first,
    key_first,
    value_first,
    query_second,
    key_second,
    value_second,
    mix_lambda,
    head_gain,
    out_weight,
    residual,
    norm_gain,
    up_weight,
    down_weight,
):
    up_whole, down_whole = rows_first((up_weight, down_weight), "sp", (0, 1))
    tok_dev, local_heads, width_first = query_first.shape
    size_first = width_first // 2
    size_second = query_second.shape[2] // 2
    value_size = value_first.shape[2]
    scale_first = 1.0 / math.sqrt(size_first)
    scale_second = 1.0 / math.sqrt(size_second)
    queries_first = query_first.reshape(tok_dev, local_heads, 2, size_first)
    queries_second = query_second.reshape(tok_dev, local_heads, 2, size_second)

    def initial():
        return (
            jnp.full((local_heads, 2, tok_dev), LOWEST, jnp.float32),
            jnp.zeros((local_heads, 2, tok_dev), jnp.float32),
            jnp.zeros((local_heads, 2, tok_dev, value_size), jnp.float32),
        )

    carried = (initial(), initial())
    pieces = side_by_side((key_first, key_second, value_first, value_second), "sp", 0, 2)
    length = pieces[0].shape[0]
    block_count = length // tok_dev
    segments = tuple(
        (member.reshape((block_count, tok_dev) + member.shape[1:]) for member in pieces)
    )

    def absorb_block(running, segment):
        keys_one, keys_two, values_one, values_two = segment
        first_state = fold_group(
            running[0],
            queries_first,
            keys_one.reshape(tok_dev, local_heads, 2, size_first),
            values_one,
            scale_first,
        )
        second_state = fold_group(
            running[1],
            queries_second,
            keys_two.reshape(tok_dev, local_heads, 2, size_second),
            values_two,
            scale_second,
        )
        return ((first_state, second_state), None)

    carried, unused = lax.scan(absorb_block, carried, segments)
    state_first, state_second = carried
    heads_first = finish_group(state_first, mix_lambda[0], head_gain[0])
    heads_second = finish_group(state_second, mix_lambda[1], head_gain[1])
    stacked = jnp.stack([heads_first, heads_second])
    selected = stacked
    projected = sum_at_owner(
        jnp.einsum(
            "ghqv,ghvd->qd", selected, out_weight, preferred_element_type=jnp.float32
        ).astype(jnp.bfloat16),
        "tp",
        0,
    ) + residual.astype(jnp.float32)
    normed = layer_norm(projected, norm_gain[0])
    mixer_in = lax.all_gather(normed.astype(jnp.bfloat16), "tp", axis=0, tiled=True)
    hidden = squared_relu(jnp.dot(mixer_in, up_whole, preferred_element_type=jnp.float32))
    selected = hidden
    mixed_sum = lax.psum_scatter(
        jnp.dot(selected, down_whole, preferred_element_type=jnp.float32).astype(jnp.bfloat16),
        "tp",
        scatter_dimension=0,
        tiled=True,
    ).astype(jnp.float32)
    return layer_norm(normed + mixed_sum, norm_gain[1]).astype(jnp.bfloat16)


def solution(mesh):
    return jax.shard_map(
        local,
        mesh=mesh,
        in_specs=(
            P("sp", "tp", None),
            P("sp", "tp", None),
            P("sp", "tp", None),
            P("sp", "tp", None),
            P("sp", "tp", None),
            P("sp", "tp", None),
            P(None, "tp"),
            P(None, "tp", None),
            P(None, "tp", None, None),
            P(("sp", "tp"), None),
            P(),
            P("sp", "tp"),
            P("tp", "sp"),
        ),
        out_specs=P(("sp", "tp"), None),
        check_vma=False,
    )
```

profile of v0, /device:TPU:1, one launch (start us, length us, event | category | flops | bytes accessed | tf_op | source)
XLA Modules:
  0.0 478.5 jit_solution(11689193848583894708)
XLA Ops:
  6.6 2.4 pad_maximum_fusion
  15.6 103.0 %all-gather.4.cloned.1.call-done = bf16[12288,1,640]{2,0,1:T(8,128)(2,1)} async-done(((bf16[768,1,640]{2,0,1:T(8,128)(2,1)}), bf16[12288,1,640]{2,0,1:T(8,128)(2,1)}) %all-gather.4.cloned.1.call-update) | async-done | bytes 15728656 | tf_op jit(solution)/shard_map/all_gather | solution.py:25
  118.5 6.9 %fusion.68 = (bf16[12288,1,128]{2,0,1:T(8,128)(2,1)}, bf16[12288,1,128]{2,0,1:T(8,128)(2,1)}, bf16[12288,1,128]{2,0,1:T(8,128)(2,1)}) fusion(bf16[12288,1,640]{2,0,1:T(8,128)(2,1)} %all-gather.4.cloned.1.call-done), kind=kLoop, calls=%fused_computation.104 | loop fusion | bytes 18874368 | tf_op jit(solution)/shard_map/slice | solution.py:27
  125.5 6.5 %slice.82 = bf16[12288,1,256]{2,0,1:T(8,128)(2,1)} slice(bf16[12288,1,640]{2,0,1:T(8,128)(2,1)} %all-gather.4.cloned.1.call-done), slice={[0:12288], [0:1], [128:384]} | slice | bytes 12582912 | tf_op jit(solution)/shard_map/slice | solution.py:27
  132.0 213.0 %while.21 = (s32[]{:T(128)}, f32[1,2,768]{2,1,0:T(2,128)S(1)}, f32[1,2,768]{2,1,0:T(2,128)S(1)}, f32[1,2,768,128]{3,2,1,0:T(8,128)S(1)}, f32[1,2,768]{2,1,0:T(2,...) while((s32[]{:T(128)}, f32[1,2,768]{2,1,0:T(2,128)S(1)}, ...), condition=%wide.region_5.6_spmd.clone, body=%wide.region_0.5_spmd.clone.sunk | while | flops 1077037056 | bytes 69403912 | solution.py:139
  135.1 2.1 copy-done.1
  137.2 2.1 fusion.98
  141.3 2.3 fusion.97
  148.4 2.1 copy-done.1
  150.5 2.1 fusion.98
  154.6 2.3 fusion.97
  159.9 1.9 bitcast_reduce_fusion.5
  161.8 2.1 copy-done.1
  163.8 2.1 fusion.98
  168.0 2.3 fusion.97
  175.1 2.1 copy-done.1
  177.2 2.1 fusion.98
  181.3 2.3 fusion.97
  186.5 1.9 bitcast_reduce_fusion.5
  188.4 2.1 copy-done.1
  190.5 2.1 fusion.98
  194.7 2.3 fusion.97
  201.7 2.1 copy-done.1
  203.8 2.1 fusion.98
  208.0 2.3 fusion.97
  215.0 2.1 copy-done.1
  217.1 2.1 fusion.98
  221.3 2.3 fusion.97
  228.3 2.1 copy-done.1
  230.4 2.1 fusion.98
  234.6 2.3 fusion.97
  241.7 2.1 copy-done.1
  243.7 2.1 fusion.98
  247.9 2.3 fusion.97
  255.0 2.1 copy-done.1
  257.0 2.1 fusion.98
  261.2 2.3 fusion.97
  268.3 2.1 copy-done.1
  270.3 2.1 fusion.98
  274.5 2.3 fusion.97
  281.6 2.1 copy-done.1
  283.7 2.1 fusion.98
  287.8 2.3 fusion.97
  294.9 2.1 copy-done.1
  297.0 2.1 fusion.98
  301.1 2.3 fusion.97
  308.2 2.1 copy-done.1
  310.3 2.1 fusion.98
  314.4 2.3 fusion.97
  321.5 2.1 copy-done.1
  323.6 2.1 fusion.98
  327.7 2.3 fusion.97
  334.8 2.1 copy-done.1
  336.9 2.1 fusion.98
  341.0 2.3 fusion.97
  347.2 2.1 fusion.57
  349.4 2.7 bitcast_convert_fusion
  352.1 5.3 %all-to-all-start = ((bf16[8,96,2048]{2,1,0:T(8,128)(2,1)}), bf16[8,96,2048]{2,1,0:T(8,128)(2,1)}, u32[]{:S(2)}, u32[]{:S(2)}) async-start(bf16[8,96,2048]{2,1,0:T(8,128)(2,1)} %bitcast.201), calls=%async_computation | async-start | bytes 6291456 | tf_op jit(solution)/shard_map/all_to_all | solution.py:40
  357.4 37.5 %all-to-all-done = bf16[8,96,2048]{2,1,0:T(8,128)(2,1)} async-done(((bf16[8,96,2048]{2,1,0:T(8,128)(2,1)}), bf16[8,96,2048]{2,1,0:T(8,128)(2,1)}, u32[]{:S(2)}, u32[]{:S(2)}) %all-to-all-start) | async-done | bytes 3145760 | tf_op jit(solution)/shard_map/all_to_all | solution.py:40
  394.9 2.5 convert_reduce_fusion
  399.1 26.0 %all-gather.6.cloned.1.call-done = bf16[768,2048]{1,0:T(8,128)(2,1)} async-done(((bf16[96,2048]{1,0:T(8,128)(2,1)}), bf16[768,2048]{1,0:T(8,128)(2,1)}) %all-gather.6.cloned.1.call-update) | async-done | bytes 3145744 | tf_op jit(solution)/shard_map/all_gather | solution.py:153
  425.1 6.7 %multiply_convert_fusion = bf16[768,1024]{1,0:T(8,128)(2,1)S(1)} fusion(bf16[768,2048]{1,0:T(8,128)(2,1)} %all-gather.6.cloned.1.call-done, bf16[2048,2048]{0,1:T(8,128)(2,1)} %all-gather.8.cloned.1.call-done), kind=kOutput, calls=%fused_computation.55 | convolution fusion | flops 3223584768 | bytes 8912896 | tf_op jit(solution)/shard_map/dot_general | solution.py:154
  431.9 4.8 %fusion.44 = bf16[768,2048]{1,0:T(8,128)(2,1)} fusion(bf16[768,1024]{1,0:T(8,128)(2,1)S(1)} %multiply_convert_fusion, bf16[2048,2048]{0,1:T(8,128)(2,1)S(1)} %copy-done.8), kind=kOutput, calls=%fused_computation.54 | convolution fusion | flops 3222798336 | bytes 8912896 | tf_op jit(solution)/shard_map/dot_general | solution.py:157
  436.7 32.7 %reduce-scatter.2.cloned.1.call-done = bf16[96,2048]{1,0:T(8,128)(2,1)} async-done(((bf16[768,2048]{1,0:T(8,128)(2,1)}), bf16[96,2048]{1,0:T(8,128)(2,1)}) %reduce-scatter.2.cloned.1.call-update) | async-done | bytes 393232 | tf_op jit(solution)/shard_map/reduce_scatter | solution.py:156
  (387 shorter events, 115.3 us)
Async XLA Ops:
  6.5 342.8 %copy-start = (bf16[2,1,128,2048]{3,2,1,0:T(8,128)(2,1)S(1)}, bf16[2,1,128,2048]{3,2,1,0:T(8,128)(2,1)}, u32[]{:S(2)}) copy-start(bf16[2,1,128,2048]{3,2,1,0:T(8,128)(2,1)} %param.23) | copy-start | bytes 3145732
  6.5 5.5 %copy-start.4 = (bf16[768,1,256]{2,0,1:T(8,128)(2,1)S(1)}, bf16[768,1,256]{2,0,1:T(8,128)(2,1)}, u32[]{:S(2)}) copy-start(bf16[768,1,256]{2,0,1:T(8,128)(2,1)} %param.18) | copy-start | bytes 1179652
  6.5 8.4 %copy-start.6 = (f32[2,1]{0,1:T(1,128)S(1)}, f32[2,1]{0,1:T(1,128)}, u32[]{:S(2)}) copy-start(f32[2,1]{0,1:T(1,128)} %param.21) | copy-start | bytes 28
  6.5 9.0 %copy-start.7 = (f32[2,1,128]{2,1,0:T(1,128)S(1)}, f32[2,1,128]{2,1,0:T(1,128)}, u32[]{:S(2)}) copy-start(f32[2,1,128]{2,1,0:T(1,128)} %param.22) | copy-start | bytes 3076
  6.5 112.0 %all-gather.4.cloned.1.call-start = ((), (), s32[]{:S(2)}) async-start(), calls=%async_computation.2 | async-start | bytes 16711680 | tf_op jit(solution)/shard_map/all_gather | solution.py:25
  9.0 390.1 %all-gather.8.cloned.1.call-start = ((), (), s32[]{:S(2)}) async-start(), calls=%async_computation.4 | async-start | bytes 8912896 | tf_op jit(solution)/shard_map/all_gather | solution.py:15
  135.1 2.1 copy-start.1
  135.1 5.4 %copy-start.2 = (bf16[768,1,2,64]{0,3,2,1:T(8,128)(2,1)S(1)}, bf16[768,1,2,64]{0,3,2,1:T(8,128)(2,1)}, u32[]{:S(2)}) copy-start(bf16[768,1,2,64]{0,3,2,1:T(8,128)(2,1)} %get-tuple-element.324) | copy-start | bytes 589828 | tf_op jit(solution)/shard_map/while
  141.3 3.1 slice-start
  141.3 3.1 slice-start.1
  148.4 2.1 copy-start.1
  148.4 5.4 %copy-start.2 = (bf16[768,1,2,64]{0,3,2,1:T(8,128)(2,1)S(1)}, bf16[768,1,2,64]{0,3,2,1:T(8,128)(2,1)}, u32[]{:S(2)}) copy-start(bf16[768,1,2,64]{0,3,2,1:T(8,128)(2,1)} %get-tuple-element.324) | copy-start | bytes 589828 | tf_op jit(solution)/shard_map/while
  154.6 3.1 slice-start
  154.6 3.1 slice-start.1
  161.7 5.4 %copy-start.2 = (bf16[768,1,2,64]{0,3,2,1:T(8,128)(2,1)S(1)}, bf16[768,1,2,64]{0,3,2,1:T(8,128)(2,1)}, u32[]{:S(2)}) copy-start(bf16[768,1,2,64]{0,3,2,1:T(8,128)(2,1)} %get-tuple-element.324) | copy-start | bytes 589828 | tf_op jit(solution)/shard_map/while
  168.0 3.1 slice-start
  168.0 3.1 slice-start.1
  175.0 2.1 copy-start.1
  175.1 5.4 %copy-start.2 = (bf16[768,1,2,64]{0,3,2,1:T(8,128)(2,1)S(1)}, bf16[768,1,2,64]{0,3,2,1:T(8,128)(2,1)}, u32[]{:S(2)}) copy-start(bf16[768,1,2,64]{0,3,2,1:T(8,128)(2,1)} %get-tuple-element.324) | copy-start | bytes 589828 | tf_op jit(solution)/shard_map/while
  181.3 3.1 slice-start
  181.3 3.1 slice-start.1
  188.4 5.4 %copy-start.2 = (bf16[768,1,2,64]{0,3,2,1:T(8,128)(2,1)S(1)}, bf16[768,1,2,64]{0,3,2,1:T(8,128)(2,1)}, u32[]{:S(2)}) copy-start(bf16[768,1,2,64]{0,3,2,1:T(8,128)(2,1)} %get-tuple-element.324) | copy-start | bytes 589828 | tf_op jit(solution)/shard_map/while
  194.6 3.1 slice-start
  194.6 3.1 slice-start.1
  201.7 5.4 %copy-start.2 = (bf16[768,1,2,64]{0,3,2,1:T(8,128)(2,1)S(1)}, bf16[768,1,2,64]{0,3,2,1:T(8,128)(2,1)}, u32[]{:S(2)}) copy-start(bf16[768,1,2,64]{0,3,2,1:T(8,128)(2,1)} %get-tuple-element.324) | copy-start | bytes 589828 | tf_op jit(solution)/shard_map/while
  207.9 3.1 slice-start
  208.0 3.1 slice-start.1
  215.0 5.4 %copy-start.2 = (bf16[768,1,2,64]{0,3,2,1:T(8,128)(2,1)S(1)}, bf16[768,1,2,64]{0,3,2,1:T(8,128)(2,1)}, u32[]{:S(2)}) copy-start(bf16[768,1,2,64]{0,3,2,1:T(8,128)(2,1)} %get-tuple-element.324) | copy-start | bytes 589828 | tf_op jit(solution)/shard_map/while
  221.2 3.1 slice-start
  221.3 3.1 slice-start.1
  228.3 5.4 %copy-start.2 = (bf16[768,1,2,64]{0,3,2,1:T(8,128)(2,1)S(1)}, bf16[768,1,2,64]{0,3,2,1:T(8,128)(2,1)}, u32[]{:S(2)}) copy-start(bf16[768,1,2,64]{0,3,2,1:T(8,128)(2,1)} %get-tuple-element.324) | copy-start | bytes 589828 | tf_op jit(solution)/shard_map/while
  234.6 3.1 slice-start
  234.6 3.1 slice-start.1
  241.6 2.1 copy-start.1
  241.6 5.4 %copy-start.2 = (bf16[768,1,2,64]{0,3,2,1:T(8,128)(2,1)S(1)}, bf16[768,1,2,64]{0,3,2,1:T(8,128)(2,1)}, u32[]{:S(2)}) copy-start(bf16[768,1,2,64]{0,3,2,1:T(8,128)(2,1)} %get-tuple-element.324) | copy-start | bytes 589828 | tf_op jit(solution)/shard_map/while
  247.9 3.1 slice-start
  247.9 3.1 slice-start.1
  254.9 5.4 %copy-start.2 = (bf16[768,1,2,64]{0,3,2,1:T(8,128)(2,1)S(1)}, bf16[768,1,2,64]{0,3,2,1:T(8,128)(2,1)}, u32[]{:S(2)}) copy-start(bf16[768,1,2,64]{0,3,2,1:T(8,128)(2,1)} %get-tuple-element.324) | copy-start | bytes 589828 | tf_op jit(solution)/shard_map/while
  261.2 3.1 slice-start
  261.2 3.1 slice-start.1
  268.2 5.4 %copy-start.2 = (bf16[768,1,2,64]{0,3,2,1:T(8,128)(2,1)S(1)}, bf16[768,1,2,64]{0,3,2,1:T(8,128)(2,1)}, u32[]{:S(2)}) copy-start(bf16[768,1,2,64]{0,3,2,1:T(8,128)(2,1)} %get-tuple-element.324) | copy-start | bytes 589828 | tf_op jit(solution)/shard_map/while
  274.5 3.1 slice-start
  274.5 3.1 slice-start.1
  281.5 5.4 %copy-start.2 = (bf16[768,1,2,64]{0,3,2,1:T(8,128)(2,1)S(1)}, bf16[768,1,2,64]{0,3,2,1:T(8,128)(2,1)}, u32[]{:S(2)}) copy-start(bf16[768,1,2,64]{0,3,2,1:T(8,128)(2,1)} %get-tuple-element.324) | copy-start | bytes 589828 | tf_op jit(solution)/shard_map/while
  287.8 3.1 slice-start
  287.8 3.1 slice-start.1
  294.8 5.4 %copy-start.2 = (bf16[768,1,2,64]{0,3,2,1:T(8,128)(2,1)S(1)}, bf16[768,1,2,64]{0,3,2,1:T(8,128)(2,1)}, u32[]{:S(2)}) copy-start(bf16[768,1,2,64]{0,3,2,1:T(8,128)(2,1)} %get-tuple-element.324) | copy-start | bytes 589828 | tf_op jit(solution)/shard_map/while
  301.1 3.1 slice-start
  301.1 3.1 slice-start.1
  308.1 5.4 %copy-start.2 = (bf16[768,1,2,64]{0,3,2,1:T(8,128)(2,1)S(1)}, bf16[768,1,2,64]{0,3,2,1:T(8,128)(2,1)}, u32[]{:S(2)}) copy-start(bf16[768,1,2,64]{0,3,2,1:T(8,128)(2,1)} %get-tuple-element.324) | copy-start | bytes 589828 | tf_op jit(solution)/shard_map/while
  314.4 3.1 slice-start
  314.4 3.1 slice-start.1
  321.5 5.4 %copy-start.2 = (bf16[768,1,2,64]{0,3,2,1:T(8,128)(2,1)S(1)}, bf16[768,1,2,64]{0,3,2,1:T(8,128)(2,1)}, u32[]{:S(2)}) copy-start(bf16[768,1,2,64]{0,3,2,1:T(8,128)(2,1)} %get-tuple-element.324) | copy-start | bytes 589828 | tf_op jit(solution)/shard_map/while
  327.7 3.1 slice-start
  327.7 3.1 slice-start.1
  334.8 5.4 %copy-start.2 = (bf16[768,1,2,64]{0,3,2,1:T(8,128)(2,1)S(1)}, bf16[768,1,2,64]{0,3,2,1:T(8,128)(2,1)}, u32[]{:S(2)}) copy-start(bf16[768,1,2,64]{0,3,2,1:T(8,128)(2,1)} %get-tuple-element.324) | copy-start | bytes 589828 | tf_op jit(solution)/shard_map/while
  341.0 3.1 slice-start
  341.0 3.1 slice-start.1
  352.1 5.3 %copy-start.5 = (f32[2,2048]{1,0:T(2,128)S(1)}, f32[2,2048]{1,0:T(2,128)}, u32[]{:S(2)}) copy-start(f32[2,2048]{1,0:T(2,128)} %param.25) | copy-start | bytes 49156
  352.1 45.4 %copy-start.3 = (bf16[96,2048]{1,0:T(8,128)(2,1)S(1)}, bf16[96,2048]{1,0:T(8,128)(2,1)}, u32[]{:S(2)}) copy-start(bf16[96,2048]{1,0:T(8,128)(2,1)} %param.24) | copy-start | bytes 1179652
  352.1 42.9 %all-to-all-start = ((bf16[8,96,2048]{2,1,0:T(8,128)(2,1)}), bf16[8,96,2048]{2,1,0:T(8,128)(2,1)}, u32[]{:S(2)}, u32[]{:S(2)}) async-start(bf16[8,96,2048]{2,1,0:T(8,128)(2,1)} %bitcast.201), calls=%async_computation | async-start | bytes 6291456 | tf_op jit(solution)/shard_map/all_to_all | solution.py:40
  357.4 67.8 %all-gather.6.cloned.1.call-start = ((), (), s32[]{:S(2)}) async-start(), calls=%async_computation.3 | async-start | bytes 3538944 | tf_op jit(solution)/shard_map/all_gather | solution.py:153
  398.9 70.5 %reduce-scatter.2.cloned.1.call-start = ((), (), s32[]{:S(2)}) async-start(), calls=%async_computation.5 | async-start | bytes 3538944 | tf_op jit(solution)/shard_map/reduce_scatter | solution.py:156
  425.1 6.7 %copy-start.8 = (bf16[2048,2048]{0,1:T(8,128)(2,1)S(1)}, bf16[2048,2048]{0,1:T(8,128)(2,1)}, u32[]{:S(2)}) copy-start(bf16[2048,2048]{0,1:T(8,128)(2,1)} %all-gather.8.cloned.1.call-done) | copy-start | bytes 25165828
  (12 other events, 25.5 us)
Sparse Core Ops, SparseCore 0:
  9.5 108.9 all-gather.3
  120.6 75.7 all-gather.7
  399.0 26.0 all-gather.5
  436.8 32.5 reduce-scatter.1
where the time goes:
time: 483 us; the launch traced here: 479 us
  waiting for transfers between devices  199 us (41%)
  matrix products  128 us (27%)
  local copies, waits for them, and re-layouts  88.6 us (18%)
  other arithmetic  41.1 us (9%)
  between operations  13.3 us (3%)
  starting transfers between devices  5.59 us (1%)
    all_gather x1, waiting for transfers between devices, side_by_side(): lax.all_gather(both, axis, axis=dim, tiled=True)  103 us
    dot_general x32, matrix products, fold_group(): jnp.einsum('hcqp,phv->hcqv', weights.astype(jnp.bfloat16), values, prefer...  71.2 us
    dot_general x32, matrix products, fold_group(): jnp.einsum('qhck,phck->hcqp', queries, key_rows, preferred_element_type=j...  42.9 us
    all_to_all x1, waiting for transfers between devices, sum_at_owner(): lax.all_to_all(parts, axis, split_axis=0, concat_axis=0, tiled=True)  37.5 us
    dynamic_slice x64, local copies, waits for them, and re-layouts, local(): carried, unused = lax.scan(absorb_block, carried, segments)  36.7 us
    while x160, local copies, waits for them, and re-layouts  33.7 us
    reduce_scatter x1, waiting for transfers between devices, local(): lax.psum_scatter(jnp.dot(selected, down_whole, preferred_element_type=jnp...  32.7 us
    all_gather x1, waiting for transfers between devices, local(): lax.all_gather(normed.astype(jnp.bfloat16), 'tp', axis=0, tiled=True)  26 us
  transfers between devices with their start and end apart: 5, of which 4 were waited for; matrix products, arithmetic and copies ran while one was open for 43% of the time, Pallas kernels for 0%

commit v1 on v0

v1 whole, which is shorter than its diff:
```python
import functools
import math

import jax
import jax.numpy as jnp
from jax import lax
from jax.experimental import pallas as pl
from jax.experimental.pallas import tpu as pltpu
from jax.sharding import PartitionSpec as P

EPSILON = 1e-05
LOWEST = -1e30
LOG2E = math.log2(math.e)
MESH = pl.DeviceIdType.MESH
BF16 = jnp.bfloat16
F32 = jnp.float32

TOK = 768
OWN = 96
SIZE = 128
VALUE = 128
SLAB = TOK + VALUE * TOK // 256
TILE = 512
TILES = 2 * TOK // TILE
ROWS = VALUE + 16


def attention_kernel(q_ref, kv_ref, prm_ref, out_ref, q_all, kv_all, prm_all, s0, s1, top, acc, heads, got,
                     q_send, kv_send, prm_send, right_send, left_send, side_send, head_send,
                     q_recv, kv_recv, prm_recv, head_recv):
    sp, tp = lax.axis_index("sp"), lax.axis_index("tp")
    z, y = lax.div(sp, 4), lax.rem(sp, 4)
    x, c = lax.div(tp, 2), lax.rem(tp, 2)

    def at(z_, y_, x_, c_):
        return {"sp": z_ * 4 + y_, "tp": x_ * 2 + c_}

    above, below = lax.rem(z + 1, 4), lax.rem(z + 3, 4)
    far = lax.rem(z + 2, 4)
    right, left, side = at(above, y, x, c), at(below, y, x, c), at(z, y, x, 1 - c)

    barrier = pltpu.get_barrier_semaphore()

    def greet(i, carry):
        other = lax.rem(y * 8 + tp + i, 32)
        pl.semaphore_signal(barrier, inc=1, device_id={"sp": z * 4 + lax.div(other, 8), "tp": lax.rem(other, 8)},
                            device_id_type=MESH)
        return carry

    lax.fori_loop(1, 32, greet, 0)
    pl.semaphore_signal(barrier, inc=1, device_id=right, device_id_type=MESH)
    pl.semaphore_signal(barrier, inc=1, device_id=left, device_id_type=MESH)
    pl.semaphore_wait(barrier, 33)

    def remote(src, dst, send, recv, device):
        return pltpu.make_async_remote_copy(src_ref=src, dst_ref=dst, send_sem=send, recv_sem=recv, device_id=device,
                                            device_id_type=MESH)

    half = lax.div(y, 2)
    slot_j = lax.rem(y, 2)

    def spread(g):
        u = 2 * c + g
        to = at(z, u, x, half)
        lanes = pl.ds(pl.multiple_of(slot_j * TOK, TOK), TOK)
        return (
            (q_ref.at[g], q_all.at[:, :, lanes], q_send.at[g], q_recv.at[slot_j], to),
            (prm_ref.at[g], prm_all.at[slot_j], prm_send.at[g], prm_recv.at[slot_j], to),
            (kv_ref.at[g], kv_all.at[z * 4 + y], kv_send.at[g], kv_recv.at[z * 4 + y], to),
        )

    for part in range(3):
        for g in range(2):
            src, dst, send, recv, to = spread(g)[part]
            mine = 2 * c + g == y

            @pl.when(mine)
            def _():
                pltpu.make_async_copy(src, dst, recv).start()

            @pl.when(jnp.logical_not(mine))
            def _():
                remote(src, dst, send, recv, to).start()

    def arrive(slot):
        remote(kv_all.at[slot], kv_all.at[slot], kv_send.at[0], kv_recv.at[slot], side).wait_recv()

    def to_side(slot, n):
        return remote(kv_all.at[slot], kv_all.at[slot], side_send.at[n], kv_recv.at[slot], side)

    def to_right(slot, n):
        return remote(kv_all.at[slot], kv_all.at[slot], right_send.at[n], kv_recv.at[slot], right)

    def to_left(slot, n):
        return remote(kv_all.at[slot], kv_all.at[slot], left_send.at[n], kv_recv.at[slot], left)

    first = z * 4 + 2 * c
    arrive(first)
    to_right(first, 0).start()
    arrive(first + 1)
    to_left(first + 1, 0).start()
    to_right(first + 1, 1).start()
    to_left(first, 1).start()
    to_side(first, 0).start()
    to_side(first + 1, 1).start()

    def slot_of(i):
        group, r = lax.div(i, 4), lax.rem(i, 4)
        e = lax.rem(r, 2)
        core = jnp.where(r >= 2, 1 - c, c)
        near = jnp.where(e == 0, below, above)
        row = jnp.where(group == 0, z, jnp.where(group == 3, far, near))
        j = jnp.where(group == 2, 1 - e, e)
        return row * 4 + 2 * core + j

    def duty(i):
        group, r = lax.div(i, 4), lax.rem(i, 4)

        @pl.when(jnp.logical_and(r == 0, jnp.logical_and(group > 0, group < 4)))
        def _():
            for e in range(2):
                slot = slot_of(group * 4 + e)
                arrive(slot)

                @pl.when(group == 1)
                def _():
                    (to_right if e == 0 else to_left)(slot, 2).start()

                to_side(slot, group * 2 + e).start()

        @pl.when(r >= 2)
        def _():
            arrive(slot_of(i))

    for j in range(2):
        remote(q_ref.at[0], q_all.at[:, :, pl.ds(j * TOK, TOK)], q_send.at[0], q_recv.at[j], side).wait_recv()
        remote(prm_ref.at[0], prm_all.at[j], prm_send.at[0], prm_recv.at[j], side).wait_recv()

    top[...] = jnp.full(top.shape, LOWEST, F32)
    acc[...] = jnp.zeros(acc.shape, F32)
    ones = jnp.ones((ROWS - VALUE, 256), BF16)

    def scores(slot, tile, m, held):
        queries = q_all[m, :, pl.ds(pl.multiple_of(tile * TILE, TILE), TILE)]
        peak = None
        for r in range(0, TOK, TOK // 2):
            s = jnp.dot(kv_all[slot, r : r + TOK // 2, m * SIZE : (m + 1) * SIZE], queries, preferred_element_type=F32)
            held[r : r + TOK // 2] = s
            p = jnp.max(s, axis=0, keepdims=True)
            peak = p if peak is None else jnp.maximum(peak, p)
        return peak

    def absorb(slot, tile, m, held, peak):
        old = top[tile, m]
        new = jnp.maximum(old, peak)
        top[tile, m] = new
        weights = jnp.exp2(held[...] - new).astype(BF16)
        added = None
        for b in range(TOK // 256):
            values = kv_all[slot, TOK + b * VALUE : TOK + (b + 1) * VALUE, :]
            d = jnp.dot(jnp.concatenate([values, ones], axis=0), weights[b * 256 : (b + 1) * 256],
                        preferred_element_type=F32)
            added = d if added is None else added + d
        acc[tile, m] = acc[tile, m] * jnp.exp2(old - new) + added

    peak = scores(first, 0, 0, s0)

    def step(t, peak0):
        i, tile = lax.div(t, TILES), lax.rem(t, TILES)
        slot = slot_of(i)

        @pl.when(tile == TILES - 1)
        def _():
            duty(i + 1)

        peak1 = scores(slot, tile, 1, s1)
        absorb(slot, tile, 0, s0, peak0)
        later = jnp.minimum(t + 1, 16 * TILES - 1)
        peak0 = scores(slot_of(lax.div(later, TILES)), lax.rem(later, TILES), 0, s0)
        absorb(slot, tile, 1, s1, peak1)
        return peak0

    lax.fori_loop(0, 16 * TILES, step, peak)

    gain = prm_all[0, 0:1, :]
    mix = prm_all[0, 1:2, 0:1]
    for tile in range(TILES):
        a1, a2 = acc[tile, 0], acc[tile, 1]
        attended = a1[:VALUE] / a1[VALUE : VALUE + 1] - mix * (a2[:VALUE] / a2[VALUE : VALUE + 1])
        square = jnp.mean(attended * attended, axis=0, keepdims=True)
        scaled = attended * lax.rsqrt(square + EPSILON)
        heads[tile * TILE : (tile + 1) * TILE, :] = (scaled.T * gain).astype(BF16)

    unit = (2 * x + lax.div(y, 2)) * 2 + lax.rem(y, 2)

    def deliver(n):
        j, tp_ = n // 8, n % 8
        to = {"sp": z * 4 + 2 * c + j, "tp": jnp.int32(tp_)}
        mine = jnp.logical_and(2 * c + j == y, tp == tp_)
        return heads.at[pl.ds(n * OWN, OWN)], got.at[unit], head_send.at[n], head_recv.at[unit], to, mine

    for n in range(16):
        src, dst, send, recv, to, mine = deliver(n)

        @pl.when(mine)
        def _():
            pltpu.make_async_copy(src, dst, recv).start()

        @pl.when(jnp.logical_not(mine))
        def _():
            remote(src, dst, send, recv, to).start()

    for part in range(3):
        for g in range(2):
            src, dst, send, recv, to = spread(g)[part]

            @pl.when(jnp.logical_not(2 * c + g == y))
            def _():
                remote(src, dst, send, recv, to).wait_send()

    for n in range(3):
        to_right(first, n).wait_send()
        to_left(first, n).wait_send()
    for n in range(8):
        to_side(first, n).wait_send()
    for n in range(16):
        src, dst, send, recv, to, mine = deliver(n)

        @pl.when(jnp.logical_not(mine))
        def _():
            remote(src, dst, send, recv, to).wait_send()

    for n in range(16):
        remote(got.at[n], got.at[n], head_send.at[n], head_recv.at[n], side).wait_recv()
    out_ref[...] = got[...]


def attention(q, kv, prm):
    dma = pltpu.SemaphoreType.DMA
    vmem = pl.BlockSpec(memory_space=pltpu.VMEM)
    return pl.pallas_call(
        attention_kernel,
        out_shape=jax.ShapeDtypeStruct((16, OWN, VALUE), BF16),
        in_specs=[vmem] * 3,
        out_specs=vmem,
        scratch_shapes=[
            pltpu.VMEM((2, SIZE, 2 * TOK), BF16),
            pltpu.VMEM((16, SLAB, 256), BF16),
            pltpu.VMEM((2, 8, 128), F32),
            pltpu.VMEM((TOK, TILE), F32),
            pltpu.VMEM((TOK, TILE), F32),
            pltpu.VMEM((TILES, 2, 1, TILE), F32),
            pltpu.VMEM((TILES, 2, ROWS, TILE), F32),
            pltpu.VMEM((2 * TOK, VALUE), BF16),
            pltpu.VMEM((16, OWN, VALUE), BF16),
            dma((2,)), dma((2,)), dma((2,)), dma((3,)), dma((3,)), dma((8,)), dma((16,)),
            dma((2,)), dma((16,)), dma((2,)), dma((16,)),
        ],
        compiler_params=pltpu.CompilerParams(collective_id=0, has_side_effects=True, vmem_limit_bytes=36 << 20),
        cost_estimate=pl.CostEstimate(flops=4 * 768 * 12288 * 4 * 128, bytes_accessed=4 << 20, transcendentals=4 * 768 * 12288),
        name="attention",
    )(q, kv, prm)


def layer_norm(activations, scales):
    average = jnp.mean(activations, axis=-1, keepdims=True)
    centred = activations - average
    spread = jnp.mean(centred * centred, axis=-1, keepdims=True)
    return centred * lax.rsqrt(spread + EPSILON) * scales


def kernel_operands(query_first, key_first, value_first, query_second, key_second, value_second, mix_lambda, head_gain):
    first = query_first[:, 0].astype(F32) * (LOG2E / 8.0)
    high = lax.reduce_precision(first, 8, 7)
    low = first - high
    second = query_second[:, 0].astype(F32) * (LOG2E / math.sqrt(128.0))
    q = jnp.stack([
        jnp.stack([jnp.concatenate([high[:, :64], low[:, :64]], 1), jnp.concatenate([high[:, 64:], low[:, 64:]], 1)]),
        jnp.stack([second[:, :128], second[:, 128:]]),
    ]).astype(BF16)
    q = jnp.swapaxes(q, 2, 3)
    one, two = key_first[:, 0, :64], key_first[:, 0, 64:]
    keys = jnp.stack([jnp.concatenate([one, one, two, two], 1), key_second[:, 0]])
    values = jnp.stack([value_first[:, 0], value_second[:, 0]])
    values = jnp.swapaxes(values.reshape(2, 3, 256, VALUE), 2, 3).reshape(2, 3 * VALUE, 256)
    kv = jnp.concatenate([keys, values], axis=1)
    prm = jnp.concatenate([head_gain, jnp.broadcast_to(mix_lambda[:, :, None], (2, 1, 128)), jnp.zeros((2, 6, 128), F32)], axis=1)
    return q, kv, prm


def squared_relu(expanded):
    return jnp.square(jnp.maximum(expanded, 0.0)).astype(BF16)


def local(query_first, key_first, value_first, query_second, key_second, value_second, mix_lambda, head_gain, out_weight,
          residual, norm_gain, up_weight, down_weight):
    both = lax.all_gather(jnp.concatenate([up_weight, down_weight.T], axis=1), "sp", axis=0, tiled=True)
    hidden_units = up_weight.shape[1]
    out_whole = lax.all_gather(out_weight[:, 0], "tp", axis=0, tiled=False).reshape(-1, out_weight.shape[-1])
    q, kv, prm = kernel_operands(query_first, key_first, value_first, query_second, key_second, value_second, mix_lambda, head_gain)
    heads = attention(q, kv, prm)
    heads = jnp.swapaxes(heads, 0, 1).reshape(OWN, 16 * VALUE)
    projected = jnp.dot(heads, out_whole, preferred_element_type=F32) + residual.astype(F32)
    normed = layer_norm(projected, norm_gain[0])
    mixer_in = lax.all_gather(normed.astype(BF16), "tp", axis=0, tiled=True)
    hidden = squared_relu(jnp.dot(mixer_in, both[:, :hidden_units], preferred_element_type=F32))
    partial = lax.dot_general(hidden, both[:, hidden_units:], (((1,), (1,)), ((), ())), preferred_element_type=F32)
    mixed_sum = lax.psum_scatter(partial.astype(BF16), "tp", scatter_dimension=0, tiled=True).astype(F32)
    return layer_norm(normed + mixed_sum, norm_gain[1]).astype(BF16)


def solution(mesh):
    heads = P("sp", "tp", None)
    return jax.shard_map(
        local,
        mesh=mesh,
        in_specs=(heads, heads, heads, heads, heads, heads, P(None, "tp"), P(None, "tp", None), P(None, "tp", None, None),
                  P(("sp", "tp"), None), P(), P("sp", "tp"), P("tp", "sp")),
        out_specs=P(("sp", "tp"), None),
        check_vma=False,
    )
```

time: 483 us -> 233 us (0.48)
  matrix products: 128 us -> 16.5 us
  waiting for transfers between devices: 199 us -> 91.9 us
  Pallas kernels: 0 us -> 96.9 us
  local copies, waits for them, and re-layouts: 88.6 us -> 2.49 us
  other arithmetic: 41.1 us -> 8.63 us
  starting transfers between devices: 5.59 us -> 0.15 us
    dot_general x67 -> x3, matrix products: 128 us -> 16.5 us  [the longest x1 6.73 us: local(): jnp.dot(mixer_in, both[:, :hidden_units], preferred_element_type=F32)]
    pallas_call x0 -> x1, Pallas kernels: none -> 96.9 us  [attention(): pl.pallas_call(attention_kernel, out_shape=jax.ShapeDtypeStruct((16, OWN,...]
    all_gather x3, waiting for transfers between devices: 129 us -> 58.5 us  [the longest x1 30 us: local(): mixer_in = lax.all_gather(normed.astype(BF16), 'tp', axis=0, tiled=True)]
    all_to_all x1 -> x0, waiting for transfers between devices: 37.5 us -> none  [sum_at_owner(): lax.all_to_all(parts, axis, split_axis=0, concat_axis=0, tiled=True)]
    dynamic_slice x64 -> x0, local copies, waits for them, and re-layouts: 36.7 us -> none  [local(): carried, unused = lax.scan(absorb_block, carried, segments)]
    while x160 -> x0, local copies, waits for them, and re-layouts: 33.7 us -> none
    reduce_sum x35 -> x0, other arithmetic: 29.8 us -> none  [the longest x32 25.1 us: fold_group(): totals = totals * factor + jnp.sum(weights, axis=-1)]
    slice x6 -> x2, local copies, waits for them, and re-layouts: 14.2 us -> 0.04 us  [the longest x1 0.03 us: kernel_operands(): high[:, :64]]
  transfers between devices with their start and end apart: 5 -> 4, of which waited for: 4 -> 3; matrix products, arithmetic and copies ran while one was open for 43% -> 5% of each run, Pallas kernels for 0% -> 42%
where the time goes in v1:
time: 233 us; the launch traced here: 230 us
  Pallas kernels  96.9 us (42%)
  waiting for transfers between devices  91.9 us (39%)
  matrix products  16.5 us (7%)
  between operations  13.4 us (6%)
  other arithmetic  8.63 us (4%)
  local copies, waits for them, and re-layouts  2.49 us (1%)
    pallas_call x1, Pallas kernels, attention(): pl.pallas_call(attention_kernel, out_shape=jax.ShapeDtypeStruct((16, OWN,...  96.9 us
    reduce_scatter x1, waiting for transfers between devices, local(): lax.psum_scatter(partial.astype(BF16), 'tp', scatter_dimension=0, tiled=T...  32.7 us
    all_gather x1, waiting for transfers between devices, local(): mixer_in = lax.all_gather(normed.astype(BF16), 'tp', axis=0, tiled=True)  30 us
    all_gather x1, waiting for transfers between devices, local(): lax.all_gather(jnp.concatenate([up_weight, down_weight.T], axis=1), 'sp',...  28.5 us
    dot_general x1, matrix products, local(): jnp.dot(mixer_in, both[:, :hidden_units], preferred_element_type=F32)  6.73 us
    dot_general x1, matrix products, local(): jnp.dot(heads, out_whole, preferred_element_type=F32) + residual.astype(F32)  4.95 us
    dot_general x1, matrix products, local(): lax.dot_general(hidden, both[:, hidden_units:], (((1,), (1,)), ((), ())),...  4.82 us
  transfers between devices with their start and end apart: 4, of which 3 were waited for; matrix products, arithmetic and copies ran while one was open for 5% of the time, Pallas kernels for 42%

profile of v1, /device:TPU:1, one launch (start us, length us, event | category | flops | bytes accessed | tf_op | source)
XLA Modules:
  0.0 230.1 jit_solution(5312521043577804981)
XLA Ops:
  6.5 0.0 copy-start.2
  6.5 0.0 copy-start.4
  6.5 0.0 copy-start.5
  6.5 0.0 copy-start.6
  6.5 0.0 all-gather.9.cloned.1.call-start
  6.6 0.7 all-gather.9.cloned.1.call-update
  7.3 0.0 all-gather.7.cloned.1.call-start
  7.3 1.1 copy.30
  8.4 1.8 pad_maximum_fusion.1
  10.2 0.0 all-gather.7.cloned.1.call-update
  10.2 0.0 all-gather.5.cloned.1.call-start
  10.3 0.0 copy-done.2
  10.3 0.2 copy.26
  10.5 0.0 copy-done.4
  10.5 0.1 copy.25
  10.6 0.0 copy-done.5
  10.7 0.1 copy.28
  10.8 0.0 copy-done.6
  10.8 0.1 copy.27
  11.0 0.0 copy-start
  11.0 0.1 pad.4.clone
  11.1 0.1 reduce-precision_convert_fusion
  11.2 0.1 fusion.11
  11.3 0.0 copy-start.10
  11.3 0.0 copy-start.8
  11.3 0.0 copy-start.1
  11.5 0.0 copy-start.7
  11.5 0.4 copy-done
  11.9 0.1 slice_bitcast_fusion.3
  12.0 0.3 maximum_bitcast_fusion.3
  12.3 0.1 maximum_bitcast_fusion.q_ref
  12.4 0.0 copy-done.10
  12.4 0.1 broadcast_in_dim.7
  12.5 0.0 copy-done.8
  12.5 0.1 maximum_maximum_fusion.prm_ref
  12.5 0.0 copy-done.1
  12.5 0.1 pad_maximum_fusion.kv_ref
  12.6 0.0 copy-done.7
  12.6 0.0 copy-start.3
  12.7 96.9 %attention.1 = bf16[16,96,128]{2,1,0:T(8,128)(2,1)S(1)} custom-call(bf16[2,2,128,768]{3,2,1,0:T(8,128)(2,1)S(1)} %maximum_bitcast_fusion.q_ref, bf16[2,1152,256]{2,1,0:T(8,128)(2,1)S(1)} %pad_maximum_fusion.kv_ref, f32[2,8,128]{2,1,0:T(8,128)S(1)} %maximum_maximum_fusion.prm_ref), custom_call_target="tpu_custom_call" | custom-call | flops 19327352832 | bytes 4194304 | tf_op jit(solution)/shard_map/attention/pallas_call | solution.py:241
  109.6 0.0 all-gather.9.cloned.1.call-done
  109.6 0.0 copy-done.3
  109.6 4.9 %fusion.18 = (f32[96]{0:T(128)S(1)}, f32[96,2048]{1,0:T(8,128)S(1)}) fusion(bf16[96,2048]{1,0:T(8,128)(2,1)S(1)} %copy-done.3, bf16[2048,2048]{1,0:T(8,128)(2,1)} %bitcast.49, bf16[16,96,128]{2,1,0:T(8,128)(2,1)S(1)} %attention.1), kind=kOutput, calls=%fused_computation.43 | convolution fusion | flops 805896064 | bytes 9961856 | tf_op jit(solution)/shard_map/dot_general | solution.py:303
  114.6 0.2 multiply_reduce_fusion.1
  114.8 0.9 fusion.9
  115.7 0.0 all-gather.5.cloned.1.call-update
  115.8 0.0 reduce-scatter.2.cloned.1.call-start
  115.8 28.5 %all-gather.7.cloned.1.call-done = bf16[2048,2048]{0,1:T(8,128)(2,1)} async-done(((bf16[128,2048]{0,1:T(8,128)(2,1)}), bf16[2048,2048]{0,1:T(8,128)(2,1)}) %all-gather.7.cloned.1.call-update) | async-done | bytes 8388624 | tf_op jit(solution)/shard_map/all_gather | solution.py:297
  144.3 30.0 %all-gather.5.cloned.1.call-done = bf16[768,2048]{1,0:T(8,128)(2,1)} async-done(((bf16[96,2048]{1,0:T(8,128)(2,1)}), bf16[768,2048]{1,0:T(8,128)(2,1)}) %all-gather.5.cloned.1.call-update) | async-done | bytes 3145744 | tf_op jit(solution)/shard_map/all_gather | solution.py:305
  174.3 0.0 copy-start.9
  174.3 6.7 %multiply_convert_fusion = bf16[768,1024]{1,0:T(8,128)(2,1)S(1)} fusion(bf16[768,2048]{1,0:T(8,128)(2,1)} %all-gather.5.cloned.1.call-done, bf16[2048,2048]{0,1:T(8,128)(2,1)} %all-gather.7.cloned.1.call-done), kind=kOutput, calls=%fused_computation.5 | convolution fusion | flops 3223584768 | bytes 8912896 | tf_op jit(solution)/shard_map/dot_general | solution.py:306
  181.0 0.0 copy-done.9
  181.1 4.8 %fusion.4 = bf16[768,2048]{1,0:T(8,128)(2,1)} fusion(bf16[768,1024]{1,0:T(8,128)(2,1)S(1)} %multiply_convert_fusion, bf16[2048,2048]{0,1:T(8,128)(2,1)S(1)} %copy-done.9), kind=kOutput, calls=%fused_computation.4 | convolution fusion | flops 3222798336 | bytes 8912896 | tf_op jit(solution)/shard_map/dot_general | solution.py:307
  185.9 0.0 reduce-scatter.2.cloned.1.call-update
  185.9 32.7 %reduce-scatter.2.cloned.1.call-done = bf16[96,2048]{1,0:T(8,128)(2,1)} async-done(((bf16[768,2048]{1,0:T(8,128)(2,1)}), bf16[96,2048]{1,0:T(8,128)(2,1)}) %reduce-scatter.2.cloned.1.call-update) | async-done | bytes 393232 | tf_op jit(solution)/shard_map/reduce_scatter | solution.py:308
  218.6 1.3 fusion.14
  220.0 1.4 multiply_reduce_fusion
  221.4 2.1 multiply_convert_fusion.1
  (13 shorter events, 0.2 us)
Async XLA Ops:
  6.5 3.8 %copy-start.2 = (bf16[768,1,256]{2,0,1:T(8,128)(2,1)S(1)}, bf16[768,1,256]{2,0,1:T(8,128)(2,1)}, u32[]{:S(2)}) copy-start(bf16[768,1,256]{2,0,1:T(8,128)(2,1)} %param.16) | copy-start | bytes 1179652
  6.5 4.0 %copy-start.4 = (bf16[768,1,128]{2,0,1:T(8,128)(2,1)S(1)}, bf16[768,1,128]{2,0,1:T(8,128)(2,1)}, u32[]{:S(2)}) copy-start(bf16[768,1,128]{2,0,1:T(8,128)(2,1)} %param.13) | copy-start | bytes 589828
  6.5 4.1 %copy-start.5 = (bf16[768,1,128]{2,0,1:T(8,128)(2,1)S(1)}, bf16[768,1,128]{2,0,1:T(8,128)(2,1)}, u32[]{:S(2)}) copy-start(bf16[768,1,128]{2,0,1:T(8,128)(2,1)} %param.18) | copy-start | bytes 589828
  6.5 4.3 %copy-start.6 = (bf16[768,1,128]{2,0,1:T(8,128)(2,1)S(1)}, bf16[768,1,128]{2,0,1:T(8,128)(2,1)}, u32[]{:S(2)}) copy-start(bf16[768,1,128]{2,0,1:T(8,128)(2,1)} %param.15) | copy-start | bytes 589828
  6.5 103.0 %all-gather.9.cloned.1.call-start = ((), (), s32[]{:S(2)}) async-start(), calls=%async_computation.4 | async-start | bytes 9437184 | tf_op jit(solution)/shard_map/all_gather | solution.py:299
  7.3 137.0 %all-gather.7.cloned.1.call-start = ((), (), s32[]{:S(2)}) async-start(), calls=%async_computation.2 | async-start | bytes 8912896 | tf_op jit(solution)/shard_map/all_gather | solution.py:297
  10.2 164.1 %all-gather.5.cloned.1.call-start = ((), (), s32[]{:S(2)}) async-start(), calls=%async_computation.1 | async-start | bytes 3538944 | tf_op jit(solution)/shard_map/all_gather | solution.py:305
  11.0 0.9 copy-start
  11.3 1.1 copy-start.10
  11.3 1.1 copy-start.8
  11.3 1.2 copy-start.1
  11.5 1.2 copy-start.7
  12.6 96.9 %copy-start.3 = (bf16[96,2048]{1,0:T(8,128)(2,1)S(1)}, bf16[96,2048]{1,0:T(8,128)(2,1)}, u32[]{:S(2)}) copy-start(bf16[96,2048]{1,0:T(8,128)(2,1)} %param.22) | copy-start | bytes 1179652
  115.8 102.8 %reduce-scatter.2.cloned.1.call-start = ((), (), s32[]{:S(2)}) async-start(), calls=%async_computation.3 | async-start | bytes 3538944 | tf_op jit(solution)/shard_map/reduce_scatter | solution.py:308
  174.3 6.7 %copy-start.9 = (bf16[2048,2048]{0,1:T(8,128)(2,1)S(1)}, bf16[2048,2048]{0,1:T(8,128)(2,1)}, u32[]{:S(2)}) copy-start(bf16[2048,2048]{0,1:T(8,128)(2,1)} %all-gather.7.cloned.1.call-done) | copy-start | bytes 25165828
Sparse Core Ops, SparseCore 0:
  9.1 53.2 all-gather.8
  64.4 79.7 all-gather.6
  146.0 28.2 all-gather.4
  186.0 32.5 reduce-scatter.1

commit v2 on v1

--- a/solution.py
+++ b/solution.py
@@ -25,9 +25,12 @@
 ROWS = VALUE + 16
 
 
-def attention_kernel(q_ref, kv_ref, prm_ref, out_ref, q_all, kv_all, prm_all, s0, s1, top, acc, heads, got,
-                     q_send, kv_send, prm_send, right_send, left_send, side_send, head_send,
-                     q_recv, kv_recv, prm_recv, head_recv):
+def attention_kernel(q_ref, kv_ref, prm_ref, w_ref, up_ref, down_ref, residual_ref, gain_ref, out_ref, q_all, kv_all, prm_all, w_all, s0, s1, top, acc, heads, got,
+                     q_send, kv_send, prm_send, right_send, left_send, side_send, head_send, w_send,
+                     q_recv, kv_recv, prm_recv, head_recv, w_recv, w_far, w_own,
+                     up_all, down_all, tokens, normed, hidden, keep, to_sib, from_sib, to_chip, from_chip,
+                     ff_send, up_recv, down_recv, ff_far, ff_own, tok_send, tok_recv, tok_far, sib_send, sib_recv,
+                     chip_send, chip_recv):
     sp, tp = lax.axis_index("sp"), lax.axis_index("tp")
     z, y = lax.div(sp, 4), lax.rem(sp, 4)
     x, c = lax.div(tp, 2), lax.rem(tp, 2)
@@ -56,31 +59,50 @@
         return pltpu.make_async_remote_copy(src_ref=src, dst_ref=dst, send_sem=send, recv_sem=recv, device_id=device,
                                             device_id_type=MESH)
 
-    half = lax.div(y, 2)
-    slot_j = lax.rem(y, 2)
+    half, odd = lax.div(y, 2), lax.rem(y, 2)
+    home = c == half
 
     def spread(g):
-        u = 2 * c + g
-        to = at(z, u, x, half)
-        lanes = pl.ds(pl.multiple_of(slot_j * TOK, TOK), TOK)
+        to = at(z, 2 * c + g, x, half)
+        lanes = pl.ds(pl.multiple_of(odd * TOK, TOK), TOK)
         return (
-            (q_ref.at[g], q_all.at[:, :, lanes], q_send.at[g], q_recv.at[slot_j], to),
-            (prm_ref.at[g], prm_all.at[slot_j], prm_send.at[g], prm_recv.at[slot_j], to),
+            (q_ref.at[g], q_all.at[:, :, lanes], q_send.at[g], q_recv.at[odd], to),
+            (prm_ref.at[g], prm_all.at[odd], prm_send.at[g], prm_recv.at[odd], to),
             (kv_ref.at[g], kv_all.at[z * 4 + y], kv_send.at[g], kv_recv.at[z * 4 + y], to),
         )
 
+    def own(part, g):
+        src, dst, send, recv, to = spread(g)[part]
+
+        @pl.when(2 * c + g == y)
+        def _():
+            pltpu.make_async_copy(src, dst, recv).start()
+
+    def away(part, g):
+        src, dst, send, recv, to = spread(g)[part]
+
+        @pl.when(jnp.logical_not(2 * c + g == y))
+        def _():
+            remote(src, dst, send, recv, to).start()
+
     for part in range(3):
         for g in range(2):
-            src, dst, send, recv, to = spread(g)[part]
-            mine = 2 * c + g == y
-
-            @pl.when(mine)
+            own(part, g)
+    for part in range(2):
+        for g in range(2):
+            away(part, g)
+    def near_or_far(far_ones):
+        for g in range(2):
+            @pl.when(odd == (g if far_ones else 1 - g))
             def _():
-                pltpu.make_async_copy(src, dst, recv).start()
-
-            @pl.when(jnp.logical_not(mine))
-            def _():
-                remote(src, dst, send, recv, to).start()
+                away(2, g)
+
+    near_or_far(False)
+
+    def place(kind):
+        return (y, y + 1 - 2 * odd, 3 - y, lax.rem(y + 2, 4))[kind]
+
+    rows = (z, below, above, far)
 
     def arrive(slot):
         remote(kv_all.at[slot], kv_all.at[slot], kv_send.at[0], kv_recv.at[slot], side).wait_recv()
@@ -94,43 +116,190 @@
     def to_left(slot, n):
         return remote(kv_all.at[slot], kv_all.at[slot], left_send.at[n], kv_recv.at[slot], left)
 
-    first = z * 4 + 2 * c
-    arrive(first)
-    to_right(first, 0).start()
-    arrive(first + 1)
-    to_left(first + 1, 0).start()
-    to_right(first + 1, 1).start()
-    to_left(first, 1).start()
-    to_side(first, 0).start()
-    to_side(first + 1, 1).start()
+    def pass_on(kind, row):
+        slot = rows[row] * 4 + place(kind)
+        second = kind % 2
+        arrive(slot)
+        if row == 0:
+            to_right(slot, second).start()
+            to_left(slot, second).start()
+        elif row == 1 and not second:
+            to_right(slot, 2).start()
+        elif row == 2 and second:
+            to_left(slot, 2).start()
+        to_side(slot, second * 4 + row).start()
+
+    east, west = at(z, y, lax.rem(x + 1, 4), c), at(z, y, lax.rem(x + 3, 4), c)
+    head_here, head_east = 2 * x + c, 2 * lax.rem(x + 1, 4) + c
+    head_west, head_far = 2 * lax.rem(x + 3, 4) + c, 2 * lax.rem(x + 2, 4) + c
+
+    def w_copy(n):
+        full = lambda h: w_all.at[h]
+        part = lambda h, k: w_all.at[h, pl.ds(k * 128, 128)]
+        return (
+            lambda: remote(w_ref, full(head_here), w_send.at[0], w_recv.at[head_here], east),
+            lambda: remote(w_ref, full(head_here), w_send.at[1], w_recv.at[head_here], west),
+            lambda: remote(w_ref, full(head_here), w_send.at[2], w_recv.at[head_here], side),
+            lambda: remote(part(head_west, 0), part(head_west, 0), w_send.at[3], w_far.at[0], east),
+            lambda: remote(part(head_east, 1), part(head_east, 1), w_send.at[4], w_far.at[1], west),
+            lambda: remote(full(head_west), full(head_west), w_send.at[5], w_recv.at[head_west], side),
+            lambda: remote(full(head_east), full(head_east), w_send.at[6], w_recv.at[head_east], side),
+            lambda: remote(full(head_far), full(head_far), w_send.at[7], w_recv.at[head_far], side),
+        )[n]()
+
+    def w_arrive(h):
+        remote(w_all.at[h], w_all.at[h], w_send.at[0], w_recv.at[h], side).wait_recv()
+
+    forth, back = at(z, lax.rem(y + 1, 4), x, c), at(z, lax.rem(y + 3, 4), x, c)
+    y_forth, y_back, y_far = lax.rem(y + 1, 4), lax.rem(y + 3, 4), lax.rem(y + 2, 4)
+
+    def up_at(s, k=None):
+        if k is None:
+            return up_all.at[pl.ds(pl.multiple_of(s * 128, 128), 128)]
+        return up_all.at[pl.ds(pl.multiple_of(s * 128 + k * 64, 64), 64)]
+
+    def down_at(s, k=None):
+        lanes = pl.ds(pl.multiple_of(s * 128, 128), 128)
+        return down_all.at[:, lanes] if k is None else down_all.at[pl.ds(k * 512, 512), lanes]
+
+    own_refs, whole, ff_recv = (up_ref, down_ref), (up_at, down_at), (up_recv, down_recv)
+
+    def ff_first(w, k):
+        return remote(own_refs[w], whole[w](sp), ff_send.at[16 * w + k], ff_recv[w].at[sp], (right, left)[k])
+
+    def ff_half(w, k):
+        shard = whole[w]((below, above)[k] * 4 + y, k)
+        return remote(shard, shard, ff_send.at[16 * w + 2 + k], ff_far.at[2 * w + k], (right, left)[k])
+
+    def ff_column(w, row, k):
+        s = row * 4 + y
+        return remote(whole[w](s), whole[w](s), ff_send.at[16 * w + 4 + 2 * row + k], ff_recv[w].at[s], (forth, back)[k])
+
+    def ff_onward(w, n, k):
+        s = (n + 2 * k) * 4 + (y_back, y_forth)[k]
+        return remote(whole[w](s), whole[w](s), ff_send.at[16 * w + 12 + 2 * n + k], ff_recv[w].at[s], (forth, back)[k])
+
+    def ff_arrive(w, s):
+        remote(whole[w](s), whole[w](s), ff_send.at[0], ff_recv[w].at[s], side).wait_recv()
+
+    def weights_begin():
+        for w in range(2):
+            pltpu.make_async_copy(own_refs[w], whole[w](sp), ff_own.at[w]).start()
+            for k in range(2):
+                ff_first(w, k).start()
+
+    def weights_halves():
+        for w in range(2):
+            ff_arrive(w, below * 4 + y)
+            ff_half(w, 0).start()
+            ff_arrive(w, above * 4 + y)
+            ff_half(w, 1).start()
+
+    def weights_columns(w):
+        if w == 0:
+            for v in range(2):
+                for k in range(2):
+                    shard = whole[v](far * 4 + y, k)
+                    remote(shard, shard, ff_send.at[0], ff_far.at[2 * v + k], side).wait_recv()
+                pltpu.make_async_copy(own_refs[v], whole[v](sp), ff_own.at[v]).wait()
+        for n in range(2):
+            for k in range(2):
+                ff_column(w, n + 2 * k, k).start()
+        for n in range(2):
+            for k in range(2):
+                ff_column(w, n + 2 - 2 * k, k).start()
+
+    def weights_onward(w):
+        for n in range(2):
+            for k in range(2):
+                ff_arrive(w, (n + 2 * k) * 4 + (y_back, y_forth)[k])
+                ff_onward(w, n, k).start()
+
+    def weights_rest(w):
+        for n in range(2):
+            for k in range(2):
+                ff_arrive(w, (n + 2 - 2 * k) * 4 + (y_back, y_forth)[k])
+                ff_arrive(w, (n + 2 * k) * 4 + y_far)
+
+    for n in range(3):
+        w_copy(n).start()
+    pltpu.make_async_copy(w_ref, w_all.at[head_here], w_own).start()
+
+    @pl.when(home)
+    def _():
+        pass_on(0, 0)
+
+    weights_begin()
+
+    @pl.when(home)
+    def _():
+        pass_on(0, 1)
+        pass_on(0, 2)
+
+    kinds = (0, 0, 0, 0, 1, 2, 1, 1, 2, 2, 3, 1, 2, 3, 3, 3)
+    order = (0, 1, 2, 3, 0, 0, 1, 2, 1, 2, 0, 3, 3, 1, 2, 3)
+    home_duties = {1: ((0, 3),), 2: ((1, 0),), 5: ((1, 1), (1, 2)), 9: ((1, 3),)}
+    away_duties = {2: ((2, 0),), 5: ((2, 1), (2, 2)), 6: ((3, 0),), 9: ((2, 3),), 11: ((3, 1), (3, 2)), 13: ((3, 3),)}
+
+    def pick(i, table):
+        value = jnp.int32(table[0])
+        for n in range(1, 16):
+            if table[n] != table[n - 1]:
+                value = jnp.where(i >= n, table[n], value)
+        return value
 
     def slot_of(i):
-        group, r = lax.div(i, 4), lax.rem(i, 4)
-        e = lax.rem(r, 2)
-        core = jnp.where(r >= 2, 1 - c, c)
-        near = jnp.where(e == 0, below, above)
-        row = jnp.where(group == 0, z, jnp.where(group == 3, far, near))
-        j = jnp.where(group == 2, 1 - e, e)
-        return row * 4 + 2 * core + j
+        kind, row = pick(i, kinds), pick(i, order)
+        row = jnp.where(row == 0, z, jnp.where(row == 1, below, jnp.where(row == 2, above, far)))
+        spot = jnp.where(kind == 0, y, jnp.where(kind == 1, y + 1 - 2 * odd, jnp.where(kind == 2, 3 - y, lax.rem(y + 2, 4))))
+        return row * 4 + spot
 
     def duty(i):
-        group, r = lax.div(i, 4), lax.rem(i, 4)
-
-        @pl.when(jnp.logical_and(r == 0, jnp.logical_and(group > 0, group < 4)))
-        def _():
-            for e in range(2):
-                slot = slot_of(group * 4 + e)
-                arrive(slot)
-
-                @pl.when(group == 1)
-                def _():
-                    (to_right if e == 0 else to_left)(slot, 2).start()
-
-                to_side(slot, group * 2 + e).start()
-
-        @pl.when(r >= 2)
-        def _():
-            arrive(slot_of(i))
+        for n in range(16):
+            for mine, duties in ((home, home_duties), (jnp.logical_not(home), away_duties)):
+                if n in duties:
+                    @pl.when(jnp.logical_and(i == n, mine))
+                    def _():
+                        for kind, row in duties[n]:
+                            pass_on(kind, row)
+        kind = pick(i + 1, kinds)
+
+        @pl.when(jnp.logical_and(i < 15, jnp.logical_not(home) == (kind < 2)))
+        def _():
+            arrive(slot_of(i + 1))
+
+        @pl.when(i == 1)
+        def _():
+            near_or_far(True)
+
+        @pl.when(i == 2)
+        def _():
+            weights_halves()
+
+        @pl.when(i == 4)
+        def _():
+            weights_columns(0)
+
+        @pl.when(i == 8)
+        def _():
+            weights_onward(0)
+            weights_columns(1)
+
+        @pl.when(i == 3)
+        def _():
+            w_arrive(head_west)
+            w_copy(3).start()
+            w_arrive(head_east)
+            w_copy(4).start()
+            w_copy(5).start()
+            w_copy(6).start()
+
+        @pl.when(i == 7)
+        def _():
+            for k in range(2):
+                remote(w_all.at[0, pl.ds(0, 128)], w_all.at[head_far, pl.ds(k * 128, 128)], w_send.at[0], w_far.at[k],
+                       side).wait_recv()
+            w_copy(7).start()
 
     for j in range(2):
         remote(q_ref.at[0], q_all.at[:, :, pl.ds(j * TOK, TOK)], q_send.at[0], q_recv.at[j], side).wait_recv()
@@ -163,7 +332,11 @@
             added = d if added is None else added + d
         acc[tile, m] = acc[tile, m] * jnp.exp2(old - new) + added
 
-    peak = scores(first, 0, 0, s0)
+    @pl.when(jnp.logical_not(home))
+    def _():
+        arrive(slot_of(jnp.int32(0)))
+
+    peak = scores(slot_of(jnp.int32(0)), 0, 0, s0)
 
     def step(t, peak0):
         i, tile = lax.div(t, TILES), lax.rem(t, TILES)
@@ -171,7 +344,7 @@
 
         @pl.when(tile == TILES - 1)
         def _():
-            duty(i + 1)
+            duty(i)
 
         peak1 = scores(slot, tile, 1, s1)
         absorb(slot, tile, 0, s0, peak0)
@@ -210,6 +383,123 @@
         def _():
             remote(src, dst, send, recv, to).start()
 
+    weights_onward(1)
+    for n in range(4):
+        w_arrive(2 * n + 1 - c)
+    pltpu.make_async_copy(w_ref, w_all.at[head_here], w_own).wait()
+    for n in range(16):
+        remote(got.at[n], got.at[n], head_send.at[n], head_recv.at[n], side).wait_recv()
+
+    def project(n, carry):
+        columns = pl.ds(pl.multiple_of(n * 512, 512), 512)
+        total = residual_ref[:, columns].astype(F32)
+        for h in range(8):
+            pair = jnp.concatenate([got[2 * h], got[2 * h + 1]], axis=1)
+            total = total + jnp.dot(pair, w_all[h, :, columns], preferred_element_type=F32)
+        normed[:, columns] = total
+        return carry
+
+    lax.fori_loop(0, 4, project, 0)
+    for r in range(0, OWN, 32):
+        value = layer_norm(normed[r : r + 32], gain_ref[0:1])
+        normed[r : r + 32] = value
+        tokens[tp, r : r + 32] = value.astype(BF16)
+
+    def tok_copy(n):
+        t_west, t_east, t_far = 2 * lax.rem(x + 3, 4) + c, 2 * lax.rem(x + 1, 4) + c, 2 * lax.rem(x + 2, 4) + c
+        half_of = lambda t, k: tokens.at[t, pl.ds(k * 48, 48)]
+        return (
+            lambda: remote(tokens.at[tp], tokens.at[tp], tok_send.at[0], tok_recv.at[tp], east),
+            lambda: remote(tokens.at[tp], tokens.at[tp], tok_send.at[1], tok_recv.at[tp], west),
+            lambda: remote(tokens.at[tp], tokens.at[tp], tok_send.at[2], tok_recv.at[tp], side),
+            lambda: remote(half_of(t_west, 0), half_of(t_west, 0), tok_send.at[3], tok_far.at[0], east),
+            lambda: remote(half_of(t_east, 1), half_of(t_east, 1), tok_send.at[4], tok_far.at[1], west),
+            lambda: remote(tokens.at[t_west], tokens.at[t_west], tok_send.at[5], tok_recv.at[t_west], side),
+            lambda: remote(tokens.at[t_east], tokens.at[t_east], tok_send.at[6], tok_recv.at[t_east], side),
+            lambda: remote(tokens.at[t_far], tokens.at[t_far], tok_send.at[7], tok_recv.at[t_far], side),
+        )[n]()
+
+    def tok_arrive(t):
+        remote(tokens.at[t], tokens.at[t], tok_send.at[0], tok_recv.at[t], side).wait_recv()
+
+    for n in range(3):
+        tok_copy(n).start()
+    weights_rest(0)
+
+    chips = (x, lax.rem(x + 3, 4), lax.rem(x + 1, 4), lax.rem(x + 2, 4))
+
+    def feed(k):
+        chip = chips[k]
+        rows_in = (2 * chip + c, 2 * chip + 1 - c)
+
+        def up(n, carry):
+            columns = pl.ds(pl.multiple_of(n * 512, 512), 512)
+            block = jnp.concatenate([tokens[rows_in[0]], tokens[rows_in[1]]], axis=0)
+            e = jnp.maximum(jnp.dot(block, up_all[:, columns], preferred_element_type=F32), 0.0)
+            hidden[:, columns] = (e * e).astype(BF16)
+            return carry
+
+        lax.fori_loop(0, 2, up, 0)
+        if k == 0:
+            weights_rest(1)
+
+        def down(n, carry):
+            columns = pl.ds(pl.multiple_of(n * 512, 512), 512)
+            p = jnp.dot(hidden[...], down_all[:, columns], preferred_element_type=F32)
+            keep[k, :, columns] = p[:OWN]
+            to_sib[k, :, columns] = p[OWN:].astype(BF16)
+            return carry
+
+        lax.fori_loop(0, 4, down, 0)
+
+    def to_sibling(k):
+        return remote(to_sib.at[k], from_sib.at[k], sib_send.at[k], sib_recv.at[k], side)
+
+    def to_owner(k):
+        return remote(to_chip.at[k - 1], from_chip.at[k - 1], chip_send.at[k - 1], chip_recv.at[k - 1], (None, west, east, at(z, y, lax.rem(x + 2, 4), c))[k])
+
+    def chip_sum(k):
+        to_sibling(k).wait_recv()
+        for r in range(0, OWN, 32):
+            to_chip[k - 1, r : r + 32] = (keep[k, r : r + 32] + from_sib[k, r : r + 32].astype(F32)).astype(BF16)
+        to_owner(k).start()
+
+    tok_arrive(2 * x + 1 - c)
+    feed(0)
+    to_sibling(0).start()
+    west_tok, east_tok, far_tok = (2 * chips[k] + c for k in (1, 2, 3))
+    tok_arrive(west_tok)
+    tok_copy(3).start()
+    tok_copy(5).start()
+    tok_arrive(east_tok)
+    tok_copy(4).start()
+    tok_copy(6).start()
+    tok_arrive(2 * chips[1] + 1 - c)
+    feed(1)
+    to_sibling(1).start()
+    tok_arrive(2 * chips[2] + 1 - c)
+    feed(2)
+    to_sibling(2).start()
+    chip_sum(1)
+    for k in range(2):
+        spot = tokens.at[far_tok, pl.ds(k * 48, 48)]
+        remote(spot, spot, tok_send.at[0], tok_far.at[k], side).wait_recv()
+    tok_copy(7).start()
+    chip_sum(2)
+    tok_arrive(2 * chips[3] + 1 - c)
+    feed(3)
+    to_sibling(3).start()
+    chip_sum(3)
+    to_sibling(0).wait_recv()
+    for k in range(1, 4):
+        to_owner(k).wait_recv()
+    for r in range(0, OWN, 32):
+        span = slice(r, r + 32)
+        total = normed[span] + keep[0, span] + from_sib[0, span].astype(F32)
+        for k in range(3):
+            total = total + from_chip[k, span].astype(F32)
+        out_ref[span] = layer_norm(total, gain_ref[1:2]).astype(BF16)
+
     for part in range(3):
         for g in range(2):
             src, dst, send, recv, to = spread(g)[part]
@@ -218,11 +508,15 @@
             def _():
                 remote(src, dst, send, recv, to).wait_send()
 
-    for n in range(3):
-        to_right(first, n).wait_send()
-        to_left(first, n).wait_send()
+    for n in range(2):
+        to_right(0, n).wait_send()
+        to_left(0, n).wait_send()
+    to_right(0, 2).wait_send()
+    to_left(0, 2).wait_send()
     for n in range(8):
-        to_side(first, n).wait_send()
+        to_side(0, n).wait_send()
+        w_copy(n).wait_send()
+        tok_copy(n).wait_send()
     for n in range(16):
         src, dst, send, recv, to, mine = deliver(n)
 
@@ -230,36 +524,58 @@
         def _():
             remote(src, dst, send, recv, to).wait_send()
 
-    for n in range(16):
-        remote(got.at[n], got.at[n], head_send.at[n], head_recv.at[n], side).wait_recv()
-    out_ref[...] = got[...]
-
-
-def attention(q, kv, prm):
+    for w in range(2):
+        for k in range(2):
+            ff_first(w, k).wait_send()
+            ff_half(w, k).wait_send()
+            for row in range(4):
+                ff_column(w, row, k).wait_send()
+            for n in range(2):
+                ff_onward(w, n, k).wait_send()
+    for k in range(4):
+        to_sibling(k).wait_send()
+    for k in range(1, 4):
+        to_owner(k).wait_send()
+
+
+def attention(q, kv, prm, w, up, down, residual, gains):
     dma = pltpu.SemaphoreType.DMA
     vmem = pl.BlockSpec(memory_space=pltpu.VMEM)
     return pl.pallas_call(
         attention_kernel,
-        out_shape=jax.ShapeDtypeStruct((16, OWN, VALUE), BF16),
-        in_specs=[vmem] * 3,
+        out_shape=jax.ShapeDtypeStruct((OWN, 2048), BF16),
+        in_specs=[vmem] * 8,
         out_specs=vmem,
         scratch_shapes=[
             pltpu.VMEM((2, SIZE, 2 * TOK), BF16),
             pltpu.VMEM((16, SLAB, 256), BF16),
             pltpu.VMEM((2, 8, 128), F32),
+            pltpu.VMEM((8, 256, 2048), BF16),
             pltpu.VMEM((TOK, TILE), F32),
             pltpu.VMEM((TOK, TILE), F32),
             pltpu.VMEM((TILES, 2, 1, TILE), F32),
             pltpu.VMEM((TILES, 2, ROWS, TILE), F32),
             pltpu.VMEM((2 * TOK, VALUE), BF16),
             pltpu.VMEM((16, OWN, VALUE), BF16),
-            dma((2,)), dma((2,)), dma((2,)), dma((3,)), dma((3,)), dma((8,)), dma((16,)),
-            dma((2,)), dma((16,)), dma((2,)), dma((16,)),
+            dma((2,)), dma((2,)), dma((2,)), dma((3,)), dma((3,)), dma((8,)), dma((16,)), dma((8,)),
+            dma((2,)), dma((16,)), dma((2,)), dma((16,)), dma((8,)), dma((2,)), dma(()),
+            pltpu.VMEM((2048, 1024), BF16),
+            pltpu.VMEM((1024, 2048), BF16),
+            pltpu.VMEM((8, OWN, 2048), BF16),
+            pltpu.VMEM((OWN, 2048), F32),
+            pltpu.VMEM((2 * OWN, 1024), BF16),
+            pltpu.VMEM((4, OWN, 2048), F32),
+            pltpu.VMEM((4, OWN, 2048), BF16),
+            pltpu.VMEM((4, OWN, 2048), BF16),
+            pltpu.VMEM((3, OWN, 2048), BF16),
+            pltpu.VMEM((3, OWN, 2048), BF16),
+            dma((32,)), dma((16,)), dma((16,)), dma((4,)), dma((2,)), dma((8,)), dma((8,)), dma((2,)), dma((4,)), dma((4,)),
+            dma((3,)), dma((3,)),
         ],
-        compiler_params=pltpu.CompilerParams(collective_id=0, has_side_effects=True, vmem_limit_bytes=36 << 20),
+        compiler_params=pltpu.CompilerParams(collective_id=0, has_side_effects=True, vmem_limit_bytes=63 << 20),
         cost_estimate=pl.CostEstimate(flops=4 * 768 * 12288 * 4 * 128, bytes_accessed=4 << 20, transcendentals=4 * 768 * 12288),
         name="attention",
-    )(q, kv, prm)
+    )(q, kv, prm, w, up, down, residual, gains)
 
 
 def layer_norm(activations, scales):
@@ -288,25 +604,10 @@
     return q, kv, prm
 
 
-def squared_relu(expanded):
-    return jnp.square(jnp.maximum(expanded, 0.0)).astype(BF16)
-
-
 def local(query_first, key_first, value_first, query_second, key_second, value_second, mix_lambda, head_gain, out_weight,
           residual, norm_gain, up_weight, down_weight):
-    both = lax.all_gather(jnp.concatenate([up_weight, down_weight.T], axis=1), "sp", axis=0, tiled=True)
-    hidden_units = up_weight.shape[1]
-    out_whole = lax.all_gather(out_weight[:, 0], "tp", axis=0, tiled=False).reshape(-1, out_weight.shape[-1])
     q, kv, prm = kernel_operands(query_first, key_first, value_first, query_second, key_second, value_second, mix_lambda, head_gain)
-    heads = attention(q, kv, prm)
-    heads = jnp.swapaxes(heads, 0, 1).reshape(OWN, 16 * VALUE)
-    projected = jnp.dot(heads, out_whole, preferred_element_type=F32) + residual.astype(F32)
-    normed = layer_norm(projected, norm_gain[0])
-    mixer_in = lax.all_gather(normed.astype(BF16), "tp", axis=0, tiled=True)
-    hidden = squared_relu(jnp.dot(mixer_in, both[:, :hidden_units], preferred_element_type=F32))
-    partial = lax.dot_general(hidden, both[:, hidden_units:], (((1,), (1,)), ((), ())), preferred_element_type=F32)
-    mixed_sum = lax.psum_scatter(partial.astype(BF16), "tp", scatter_dimension=0, tiled=True).astype(F32)
-    return layer_norm(normed + mixed_sum, norm_gain[1]).astype(BF16)
+    return attention(q, kv, prm, out_weight.reshape(2 * VALUE, -1), up_weight, down_weight, residual, norm_gain)
 
 
 def solution(mesh):

time: 233 us -> 165 us (0.71); the launches traced: 230 us -> 165 us
  waiting for transfers between devices: 91.9 us -> 0 us
  Pallas kernels: 96.9 us -> 156 us
  matrix products: 16.5 us -> 0 us
  between operations: 13.4 us -> 0.17 us
  other arithmetic: 8.63 us -> 3.32 us
  local copies, waits for them, and re-layouts: 2.49 us -> 5.02 us
    pallas_call x1, Pallas kernels: 96.9 us -> 156 us  [attention(): pl.pallas_call(attention_kernel, out_shape=jax.ShapeDtypeStruct((OWN, 204...]
    all_gather x3 -> x0, waiting for transfers between devices: 58.5 us -> none  [the longest x1 30 us: local(): mixer_in = lax.all_gather(normed.astype(BF16), 'tp', axis=0, tiled=True)]
    reduce_scatter x1 -> x0, waiting for transfers between devices: 32.7 us -> none  [local(): lax.psum_scatter(partial.astype(BF16), 'tp', scatter_dimension=0, tiled=T...]
    dot_general x3 -> x0, matrix products: 16.5 us -> none  [the longest x1 6.73 us: local(): jnp.dot(mixer_in, both[:, :hidden_units], preferred_element_type=F32)]
    convert_element_type x2 -> x0, other arithmetic: 3.08 us -> none  [the longest x1 2.15 us: local(): return layer_norm(normed + mixed_sum, norm_gain[1]).astype(BF16)]
    reduce_sum x3 -> x0, other arithmetic: 2.97 us -> none  [the longest x2 1.65 us: layer_norm(): spread = jnp.mean(centred * centred, axis=-1, keepdims=True)]
    unnamed x25 -> x17, local copies, waits for them, and re-layouts: 1.87 us -> 4.41 us
  transfers between devices with their start and end apart: 4 -> 0, of which waited for: 3 -> 0; matrix products, arithmetic and copies ran while one was open for 5% -> 0% of each run, Pallas kernels for 42% -> 0%
where the time goes in v2:
time: 165 us
  Pallas kernels  156 us (95%)
  local copies, waits for them, and re-layouts  5.02 us (3%)
  other arithmetic  3.32 us (2%)
    pallas_call x1, Pallas kernels, attention(): pl.pallas_call(attention_kernel, out_shape=jax.ShapeDtypeStruct((OWN, 204...  156 us
    unnamed x17, local copies, waits for them, and re-layouts  4.41 us

profile of v2, /device:TPU:1, one launch (start us, length us, event | category | flops | bytes accessed | tf_op | source)
XLA Modules:
  0.0 164.9 jit_solution(4415433655393403986)
XLA Ops:
  0.0 1.1 copy.14
  1.1 0.1 reduce-precision_convert_fusion
  1.1 0.0 copy-start.2
  1.3 0.9 copy-done.2
  2.1 0.2 copy.15
  2.3 0.1 fusion.1
  2.4 0.0 copy-start
  2.5 1.0 maximum_bitcast_fusion.q_ref
  3.5 0.0 copy-done
  3.5 0.0 copy-start.3
  3.5 0.0 copy-start.4
  3.5 0.1 slice_bitcast_fusion.3
  3.6 0.0 copy-start.1
  3.6 0.3 maximum_bitcast_fusion.3
  3.9 0.5 copy-done.3
  4.4 0.1 copy.16
  4.6 0.0 copy-done.4
  4.6 0.1 copy.17
  4.8 0.0 copy-done.1
  4.8 0.0 copy-start.6
  4.8 0.0 copy-start.5
  4.8 1.1 pad_maximum_fusion.kv_ref
  5.9 0.0 copy-done.6
  5.9 0.1 broadcast_in_dim.12
  6.0 0.1 pad.2.clone
  6.1 0.0 copy-done.5
  6.1 0.7 maximum_maximum_fusion.prm_ref
  6.7 156.4 %attention.1 = bf16[96,2048]{1,0:T(8,128)(2,1)} custom-call(bf16[2,2,128,768]{3,2,1,0:T(8,128)(2,1)} %maximum_bitcast_fusion.q_ref, bf16[2,1152,256]{2,1,0:T(8,128)(2,1)} %pad_maximum_fusion.kv_ref, f32[2,8,128]{2,1,0:T(8,128)} %maximum_maximum_fusion.prm_ref, bf16[256,2048]{1,0:T(8,128)(2,1)} %bitcast.37, bf16[128,1024]{1,0:T(8,128)(2,1)} %up_ref.1, ...), custom_call_target="tpu_custom_call" | custom-call | flops 19327352832 | bytes 4194304 | tf_op jit(solution)/shard_map/attention/pallas_call | solution.py:544
  163.1 1.8 %copy.19 = bf16[96,2048]{1,0:T(8,128)(2,1)} copy(bf16[96,2048]{1,0:T(8,128)(2,1)} %attention.1) | data formatting | bytes 786432
  (8 shorter events, 0.2 us)
Async XLA Ops:
  1.1 1.0 copy-start.2
  2.4 1.1 copy-start
  3.5 0.9 copy-start.3
  3.5 1.1 copy-start.4
  3.6 1.2 copy-start.1
  4.8 1.1 copy-start.6
  4.8 1.3 copy-start.5

commit v3 on v2

--- a/solution.py
+++ b/solution.py
@@ -19,17 +19,21 @@
 OWN = 96
 SIZE = 128
 VALUE = 128
-SLAB = TOK + VALUE * TOK // 256
+HALF = TOK // 2
+KEYS = VALUE * TOK // 256
+SLAB = KEYS + TOK
+LENGTHS = (KEYS + HALF, SLAB)
 TILE = 512
 TILES = 2 * TOK // TILE
 ROWS = VALUE + 16
 
 
-def attention_kernel(q_ref, kv_ref, prm_ref, w_ref, up_ref, down_ref, residual_ref, gain_ref, out_ref, q_all, kv_all, prm_all, w_all, s0, s1, top, acc, heads, got,
+def attention_kernel(q1_ref, k1_ref, v1_ref, q2_ref, k2_ref, v2_ref, mix_ref, head_gain_ref, w_ref, up_ref, down_ref, residual_hbm,
+                     gain_ref, out_ref, q_own, kv_own, prm_own, residual_ref, residual_sem, q_all, kv_all, prm_all, w_all, s0, s1, top, acc, heads, got,
                      q_send, kv_send, prm_send, right_send, left_send, side_send, head_send, w_send,
                      q_recv, kv_recv, prm_recv, head_recv, w_recv, w_far, w_own,
                      up_all, down_all, tokens, normed, hidden, keep, to_sib, from_sib, to_chip, from_chip,
-                     ff_send, up_recv, down_recv, ff_far, ff_own, tok_send, tok_recv, tok_far, sib_send, sib_recv,
+                     ff_send, up_recv, down_recv, rest_recv, ff_far, ff_own, tok_send, tok_recv, tok_far, sib_send, sib_recv,
                      chip_send, chip_recv):
     sp, tp = lax.axis_index("sp"), lax.axis_index("tp")
     z, y = lax.div(sp, 4), lax.rem(sp, 4)
@@ -53,6 +57,20 @@
     lax.fori_loop(1, 32, greet, 0)
     pl.semaphore_signal(barrier, inc=1, device_id=right, device_id_type=MESH)
     pl.semaphore_signal(barrier, inc=1, device_id=left, device_id_type=MESH)
+    residual_copy = pltpu.make_async_copy(residual_hbm, residual_ref, residual_sem)
+    residual_copy.start()
+
+    q_own[0, 0] = (q1_ref[...].astype(F32) * (LOG2E / 8.0)).T.astype(BF16)
+    for m in range(2):
+        q_own[1, m] = (q2_ref[:, m * SIZE : (m + 1) * SIZE].astype(F32) * (LOG2E / math.sqrt(128.0))).T.astype(BF16)
+    for g, values in ((0, v1_ref), (1, v2_ref)):
+        for b in range(TOK // 256):
+            kv_own[g, b * VALUE : (b + 1) * VALUE] = values[b * 256 : (b + 1) * 256].astype(F32).T.astype(BF16)
+        prm_own[g, 0:1] = head_gain_ref[g : g + 1]
+        prm_own[g, 1:2] = jnp.broadcast_to(mix_ref[g : g + 1], (1, 128))
+    for h in range(2):
+        kv_own[0, KEYS : KEYS + HALF, h * SIZE : (h + 1) * SIZE] = k1_ref[h * HALF : (h + 1) * HALF]
+    kv_own[1, KEYS:SLAB] = k2_ref[...]
     pl.semaphore_wait(barrier, 33)
 
     def remote(src, dst, send, recv, device):
@@ -62,21 +80,20 @@
     half, odd = lax.div(y, 2), lax.rem(y, 2)
     home = c == half
 
+    def q_views(g, j):
+        lanes = pl.ds(j * TOK if isinstance(j, int) else pl.multiple_of(j * TOK, TOK), TOK)
+        return (q_own.at[0, 0], q_all.at[0, :, lanes]) if g == 0 else (q_own.at[1], q_all.at[:, :, lanes])
+
+    def slab(slot, g):
+        return kv_all.at[slot, pl.ds(0, LENGTHS[g])]
+
     def spread(g):
         to = at(z, 2 * c + g, x, half)
-        lanes = pl.ds(pl.multiple_of(odd * TOK, TOK), TOK)
         return (
-            (q_ref.at[g], q_all.at[:, :, lanes], q_send.at[g], q_recv.at[odd], to),
-            (prm_ref.at[g], prm_all.at[odd], prm_send.at[g], prm_recv.at[odd], to),
-            (kv_ref.at[g], kv_all.at[z * 4 + y], kv_send.at[g], kv_recv.at[z * 4 + y], to),
+            (*q_views(g, odd), q_send.at[g], q_recv.at[odd], to),
+            (prm_own.at[g], prm_all.at[odd], prm_send.at[g], prm_recv.at[odd], to),
+            (kv_own.at[g, pl.ds(0, LENGTHS[g])], slab(z * 4 + y, g), kv_send.at[g], kv_recv.at[z * 4 + y], to),
         )
-
-    def own(part, g):
-        src, dst, send, recv, to = spread(g)[part]
-
-        @pl.when(2 * c + g == y)
-        def _():
-            pltpu.make_async_copy(src, dst, recv).start()
 
     def away(part, g):
         src, dst, send, recv, to = spread(g)[part]
@@ -85,9 +102,6 @@
         def _():
             remote(src, dst, send, recv, to).start()
 
-    for part in range(3):
-        for g in range(2):
-            own(part, g)
     for part in range(2):
         for g in range(2):
             away(part, g)
@@ -104,30 +118,53 @@
 
     rows = (z, below, above, far)
 
+    def by_group(action):
+        for g in range(2):
+            @pl.when(odd == g)
+            def _():
+                action(g)
+
+    def arrive_of(slot, g):
+        remote(slab(slot, g), slab(slot, g), kv_send.at[0], kv_recv.at[slot], side).wait_recv()
+
     def arrive(slot):
-        remote(kv_all.at[slot], kv_all.at[slot], kv_send.at[0], kv_recv.at[slot], side).wait_recv()
-
-    def to_side(slot, n):
-        return remote(kv_all.at[slot], kv_all.at[slot], side_send.at[n], kv_recv.at[slot], side)
-
-    def to_right(slot, n):
-        return remote(kv_all.at[slot], kv_all.at[slot], right_send.at[n], kv_recv.at[slot], right)
-
-    def to_left(slot, n):
-        return remote(kv_all.at[slot], kv_all.at[slot], left_send.at[n], kv_recv.at[slot], left)
+        by_group(lambda g: arrive_of(slot, g))
+
+    def to_side(slot, n, g):
+        return remote(slab(slot, g), slab(slot, g), side_send.at[n], kv_recv.at[slot], side)
+
+    def to_right(slot, n, g):
+        return remote(slab(slot, g), slab(slot, g), right_send.at[n], kv_recv.at[slot], right)
+
+    def to_left(slot, n, g):
+        return remote(slab(slot, g), slab(slot, g), left_send.at[n], kv_recv.at[slot], left)
+
+    def own_shard(g):
+        slot = z * 4 + y
+        for sends, to in ((right_send, right), (left_send, left), (side_send, side)):
+            remote(kv_own.at[g, pl.ds(0, LENGTHS[g])], slab(slot, g), sends.at[0], kv_recv.at[slot], to).start()
+        lanes = pl.ds(pl.multiple_of(odd * TOK, TOK), TOK)
+        kv_all[slot, 0 : LENGTHS[g]] = kv_own[g, 0 : LENGTHS[g]]
+        for m in range(1 + g):
+            q_all[m, :, lanes] = q_own[g, m]
+        prm_all[odd] = prm_own[g]
 
     def pass_on(kind, row):
         slot = rows[row] * 4 + place(kind)
         second = kind % 2
-        arrive(slot)
-        if row == 0:
-            to_right(slot, second).start()
-            to_left(slot, second).start()
-        elif row == 1 and not second:
-            to_right(slot, 2).start()
-        elif row == 2 and second:
-            to_left(slot, 2).start()
-        to_side(slot, second * 4 + row).start()
+
+        def relay(g):
+            arrive_of(slot, g)
+            if row == 0:
+                to_right(slot, second, g).start()
+                to_left(slot, second, g).start()
+            elif row == 1 and not second:
+                to_right(slot, 2, g).start()
+            elif row == 2 and second:
+                to_left(slot, 2, g).start()
+            to_side(slot, second * 4 + row, g).start()
+
+        by_group(relay)
 
     east, west = at(z, y, lax.rem(x + 1, 4), c), at(z, y, lax.rem(x + 3, 4), c)
     head_here, head_east = 2 * x + c, 2 * lax.rem(x + 1, 4) + c
@@ -152,94 +189,99 @@
 
     forth, back = at(z, lax.rem(y + 1, 4), x, c), at(z, lax.rem(y + 3, 4), x, c)
     y_forth, y_back, y_far = lax.rem(y + 1, 4), lax.rem(y + 3, 4), lax.rem(y + 2, 4)
-
-    def up_at(s, k=None):
-        if k is None:
-            return up_all.at[pl.ds(pl.multiple_of(s * 128, 128), 128)]
-        return up_all.at[pl.ds(pl.multiple_of(s * 128 + k * 64, 64), 64)]
-
-    def down_at(s, k=None):
+    UP, DOWN_A, DOWN_B = 0, 1, 2
+
+    def source(p):
+        return up_ref if p == UP else down_ref.at[pl.ds(512 * (p - 1), 512)]
+
+    def shard(p, s, k=None):
+        if p == UP:
+            if k is None:
+                return up_all.at[pl.ds(pl.multiple_of(s * 128, 128), 128)]
+            return up_all.at[pl.ds(pl.multiple_of(s * 128 + k * 64, 64), 64)]
         lanes = pl.ds(pl.multiple_of(s * 128, 128), 128)
-        return down_all.at[:, lanes] if k is None else down_all.at[pl.ds(k * 512, 512), lanes]
-
-    own_refs, whole, ff_recv = (up_ref, down_ref), (up_at, down_at), (up_recv, down_recv)
-
-    def ff_first(w, k):
-        return remote(own_refs[w], whole[w](sp), ff_send.at[16 * w + k], ff_recv[w].at[sp], (right, left)[k])
-
-    def ff_half(w, k):
-        shard = whole[w]((below, above)[k] * 4 + y, k)
-        return remote(shard, shard, ff_send.at[16 * w + 2 + k], ff_far.at[2 * w + k], (right, left)[k])
-
-    def ff_column(w, row, k):
-        s = row * 4 + y
-        return remote(whole[w](s), whole[w](s), ff_send.at[16 * w + 4 + 2 * row + k], ff_recv[w].at[s], (forth, back)[k])
-
-    def ff_onward(w, n, k):
-        s = (n + 2 * k) * 4 + (y_back, y_forth)[k]
-        return remote(whole[w](s), whole[w](s), ff_send.at[16 * w + 12 + 2 * n + k], ff_recv[w].at[s], (forth, back)[k])
-
-    def ff_arrive(w, s):
-        remote(whole[w](s), whole[w](s), ff_send.at[0], ff_recv[w].at[s], side).wait_recv()
-
-    def weights_begin():
-        for w in range(2):
-            pltpu.make_async_copy(own_refs[w], whole[w](sp), ff_own.at[w]).start()
-            for k in range(2):
-                ff_first(w, k).start()
-
-    def weights_halves():
-        for w in range(2):
-            ff_arrive(w, below * 4 + y)
-            ff_half(w, 0).start()
-            ff_arrive(w, above * 4 + y)
-            ff_half(w, 1).start()
-
-    def weights_columns(w):
-        if w == 0:
-            for v in range(2):
-                for k in range(2):
-                    shard = whole[v](far * 4 + y, k)
-                    remote(shard, shard, ff_send.at[0], ff_far.at[2 * v + k], side).wait_recv()
-                pltpu.make_async_copy(own_refs[v], whole[v](sp), ff_own.at[v]).wait()
+        start = 512 * (p - 1)
+        return down_all.at[pl.ds(start, 512) if k is None else pl.ds(start + k * 256, 256), lanes]
+
+    def lines(p):
+        by_z = ((right, left), (below * 4 + y, above * 4 + y, far * 4 + y), lambda r: r * 4 + y, lambda r: r * 4 + y_back,
+                lambda r: r * 4 + y_forth, lambda r: r * 4 + y_far)
+        by_y = ((forth, back), (z * 4 + y_back, z * 4 + y_forth, z * 4 + y_far), lambda r: z * 4 + r, lambda r: below * 4 + r,
+                lambda r: above * 4 + r, lambda r: far * 4 + r)
+        return by_y + ((right, left),) if p == UP else by_z + ((forth, back),)
+
+    ff_recv = (up_recv, down_recv, rest_recv)
+
+    def piece(p, n, s, to, k=None, recv=None):
+        view = shard(p, s, k)
+        return remote(view, view, ff_send.at[16 * p + n], ff_recv[p].at[s] if recv is None else recv, to)
+
+    def ff_first(p, k):
+        return remote(source(p), shard(p, sp), ff_send.at[16 * p + k], ff_recv[p].at[sp], lines(p)[0][k])
+
+    def ff_half(p, k):
+        return piece(p, 2 + k, lines(p)[1][k], lines(p)[0][k], k, ff_far.at[2 * p + k])
+
+    def ff_column(p, r, k):
+        return piece(p, 4 + 2 * r + k, lines(p)[2](r), lines(p)[6][k])
+
+    def ff_onward(p, n, k):
+        return piece(p, 12 + 2 * n + k, lines(p)[3 + k](n + 2 * k), lines(p)[6][k])
+
+    def ff_arrive(p, s):
+        piece(p, 0, s, side).wait_recv()
+
+    def begin(p):
+        pltpu.make_async_copy(source(p), shard(p, sp), ff_own.at[p]).start()
+        for k in range(2):
+            ff_first(p, k).start()
+
+    def halves(p):
+        for k in range(2):
+            ff_arrive(p, lines(p)[1][k])
+            ff_half(p, k).start()
+
+    def gathered(p):
+        for k in range(2):
+            piece(p, 0, lines(p)[1][2], side, k, ff_far.at[2 * p + k]).wait_recv()
+        pltpu.make_async_copy(source(p), shard(p, sp), ff_own.at[p]).wait()
+
+    def columns(p, second):
         for n in range(2):
             for k in range(2):
-                ff_column(w, n + 2 * k, k).start()
+                ff_column(p, (n + 2 - 2 * k) if second else (n + 2 * k), k).start()
+
+    def onward(p):
         for n in range(2):
             for k in range(2):
-                ff_column(w, n + 2 - 2 * k, k).start()
-
-    def weights_onward(w):
+                ff_arrive(p, lines(p)[3 + k](n + 2 * k))
+                ff_onward(p, n, k).start()
+
+    def complete(p):
         for n in range(2):
             for k in range(2):
-                ff_arrive(w, (n + 2 * k) * 4 + (y_back, y_forth)[k])
-                ff_onward(w, n, k).start()
-
-    def weights_rest(w):
-        for n in range(2):
-            for k in range(2):
-                ff_arrive(w, (n + 2 - 2 * k) * 4 + (y_back, y_forth)[k])
-                ff_arrive(w, (n + 2 * k) * 4 + y_far)
-
-    for n in range(3):
-        w_copy(n).start()
-    pltpu.make_async_copy(w_ref, w_all.at[head_here], w_own).start()
+                ff_arrive(p, lines(p)[3 + k](n + 2 - 2 * k))
+        for r in range(4):
+            ff_arrive(p, lines(p)[5](r))
+
 
     @pl.when(home)
     def _():
-        pass_on(0, 0)
-
-    weights_begin()
+        by_group(own_shard)
+
+    begin(DOWN_A)
+    begin(DOWN_B)
 
     @pl.when(home)
     def _():
         pass_on(0, 1)
         pass_on(0, 2)
 
+
     kinds = (0, 0, 0, 0, 1, 2, 1, 1, 2, 2, 3, 1, 2, 3, 3, 3)
     order = (0, 1, 2, 3, 0, 0, 1, 2, 1, 2, 0, 3, 3, 1, 2, 3)
-    home_duties = {1: ((0, 3),), 2: ((1, 0),), 5: ((1, 1), (1, 2)), 9: ((1, 3),)}
-    away_duties = {2: ((2, 0),), 5: ((2, 1), (2, 2)), 6: ((3, 0),), 9: ((2, 3),), 11: ((3, 1), (3, 2)), 13: ((3, 3),)}
+    home_duties = {0: ((1, 0),), 1: ((0, 3),), 5: ((1, 1), (1, 2)), 8: ((1, 3),)}
+    away_duties = {1: ((2, 0),), 4: ((3, 0),), 5: ((2, 1), (2, 2)), 7: ((2, 3),), 9: ((3, 1), (3, 2)), 12: ((3, 3),)}
 
     def pick(i, table):
         value = jnp.int32(table[0])
@@ -268,24 +310,44 @@
         def _():
             arrive(slot_of(i + 1))
 
-        @pl.when(i == 1)
+        @pl.when(i == 0)
         def _():
             near_or_far(True)
-
-        @pl.when(i == 2)
-        def _():
-            weights_halves()
-
-        @pl.when(i == 4)
-        def _():
-            weights_columns(0)
+            begin(UP)
+            for n in range(3):
+                w_copy(n).start()
+            pltpu.make_async_copy(w_ref, w_all.at[head_here], w_own).start()
+
+        @pl.when(i == 3)
+        def _():
+            halves(DOWN_A)
+            halves(DOWN_B)
+            halves(UP)
+
+        @pl.when(i == 5)
+        def _():
+            gathered(DOWN_A)
+            columns(DOWN_A, False)
+            columns(DOWN_A, True)
+
+        @pl.when(i == 6)
+        def _():
+            gathered(DOWN_B)
+            columns(DOWN_B, False)
+            columns(DOWN_B, True)
+
+        @pl.when(i == 9)
+        def _():
+            gathered(UP)
+            columns(UP, False)
+            columns(UP, True)
+
+        @pl.when(i == 10)
+        def _():
+            onward(DOWN_A)
+            onward(DOWN_B)
 
         @pl.when(i == 8)
-        def _():
-            weights_onward(0)
-            weights_columns(1)
-
-        @pl.when(i == 3)
         def _():
             w_arrive(head_west)
             w_copy(3).start()
@@ -294,7 +356,7 @@
             w_copy(5).start()
             w_copy(6).start()
 
-        @pl.when(i == 7)
+        @pl.when(i == 12)
         def _():
             for k in range(2):
                 remote(w_all.at[0, pl.ds(0, 128)], w_all.at[head_far, pl.ds(k * 128, 128)], w_send.at[0], w_far.at[k],
@@ -302,8 +364,18 @@
             w_copy(7).start()
 
     for j in range(2):
-        remote(q_ref.at[0], q_all.at[:, :, pl.ds(j * TOK, TOK)], q_send.at[0], q_recv.at[j], side).wait_recv()
-        remote(prm_ref.at[0], prm_all.at[j], prm_send.at[0], prm_recv.at[j], side).wait_recv()
+        @pl.when(jnp.logical_not(jnp.logical_and(home, odd == j)))
+        def _():
+            by_group(lambda g: remote(*q_views(g, j), q_send.at[0], q_recv.at[j], side).wait_recv())
+            remote(prm_own.at[0], prm_all.at[j], prm_send.at[0], prm_recv.at[j], side).wait_recv()
+
+    @pl.when(odd == 0)
+    def _():
+        both = q_all[0]
+        nothing = jnp.zeros((SIZE // 2, 2 * TOK), BF16)
+        q_all[1, 0 : SIZE // 2] = nothing
+        q_all[1, SIZE // 2 : SIZE] = both[SIZE // 2 : SIZE]
+        q_all[0, SIZE // 2 : SIZE] = nothing
 
     top[...] = jnp.full(top.shape, LOWEST, F32)
     acc[...] = jnp.zeros(acc.shape, F32)
@@ -312,9 +384,12 @@
     def scores(slot, tile, m, held):
         queries = q_all[m, :, pl.ds(pl.multiple_of(tile * TILE, TILE), TILE)]
         peak = None
-        for r in range(0, TOK, TOK // 2):
-            s = jnp.dot(kv_all[slot, r : r + TOK // 2, m * SIZE : (m + 1) * SIZE], queries, preferred_element_type=F32)
-            held[r : r + TOK // 2] = s
+        for h in range(2):
+            start = KEYS + (odd * HALF if h else 0)
+            entry = m * SIZE if h == m else (odd if m else 1 - odd) * SIZE
+            keys = kv_all[slot, pl.ds(pl.multiple_of(start, HALF), HALF), pl.ds(pl.multiple_of(entry, SIZE), SIZE)]
+            s = jnp.dot(keys, queries, preferred_element_type=F32)
+            held[h * HALF : (h + 1) * HALF] = s
             p = jnp.max(s, axis=0, keepdims=True)
             peak = p if peak is None else jnp.maximum(peak, p)
         return peak
@@ -326,7 +401,7 @@
         weights = jnp.exp2(held[...] - new).astype(BF16)
         added = None
         for b in range(TOK // 256):
-            values = kv_all[slot, TOK + b * VALUE : TOK + (b + 1) * VALUE, :]
+            values = kv_all[slot, b * VALUE : (b + 1) * VALUE, :]
             d = jnp.dot(jnp.concatenate([values, ones], axis=0), weights[b * 256 : (b + 1) * 256],
                         preferred_element_type=F32)
             added = d if added is None else added + d
@@ -383,12 +458,14 @@
         def _():
             remote(src, dst, send, recv, to).start()
 
-    weights_onward(1)
+    onward(UP)
     for n in range(4):
         w_arrive(2 * n + 1 - c)
     pltpu.make_async_copy(w_ref, w_all.at[head_here], w_own).wait()
     for n in range(16):
         remote(got.at[n], got.at[n], head_send.at[n], head_recv.at[n], side).wait_recv()
+
+    residual_copy.wait()
 
     def project(n, carry):
         columns = pl.ds(pl.multiple_of(n * 512, 512), 512)
@@ -424,7 +501,7 @@
 
     for n in range(3):
         tok_copy(n).start()
-    weights_rest(0)
+    complete(UP)
 
     chips = (x, lax.rem(x + 3, 4), lax.rem(x + 1, 4), lax.rem(x + 2, 4))
 
@@ -441,7 +518,8 @@
 
         lax.fori_loop(0, 2, up, 0)
         if k == 0:
-            weights_rest(1)
+            complete(DOWN_A)
+            complete(DOWN_B)
 
         def down(n, carry):
             columns = pl.ds(pl.multiple_of(n * 512, 512), 512)
@@ -508,13 +586,15 @@
             def _():
                 remote(src, dst, send, recv, to).wait_send()
 
-    for n in range(2):
-        to_right(0, n).wait_send()
-        to_left(0, n).wait_send()
-    to_right(0, 2).wait_send()
-    to_left(0, 2).wait_send()
+    def sent(g):
+        for n in range(3):
+            to_right(0, n, g).wait_send()
+            to_left(0, n, g).wait_send()
+        for n in range(8):
+            to_side(0, n, g).wait_send()
+
+    by_group(sent)
     for n in range(8):
-        to_side(0, n).wait_send()
         w_copy(n).wait_send()
         tok_copy(n).wait_send()
     for n in range(16):
@@ -524,7 +604,7 @@
         def _():
             remote(src, dst, send, recv, to).wait_send()
 
-    for w in range(2):
+    for w in range(3):
         for k in range(2):
             ff_first(w, k).wait_send()
             ff_half(w, k).wait_send()
@@ -538,15 +618,20 @@
         to_owner(k).wait_send()
 
 
-def attention(q, kv, prm, w, up, down, residual, gains):
+def layer(*operands):
     dma = pltpu.SemaphoreType.DMA
-    vmem = pl.BlockSpec(memory_space=pltpu.VMEM)
+    vmem, hbm = pl.BlockSpec(memory_space=pltpu.VMEM), pl.BlockSpec(memory_space=pl.ANY)
     return pl.pallas_call(
         attention_kernel,
         out_shape=jax.ShapeDtypeStruct((OWN, 2048), BF16),
-        in_specs=[vmem] * 8,
+        in_specs=[vmem] * 8 + [hbm] * 4 + [vmem],
         out_specs=vmem,
         scratch_shapes=[
+            pltpu.VMEM((2, 2, SIZE, TOK), BF16),
+            pltpu.VMEM((2, SLAB, 256), BF16),
+            pltpu.VMEM((2, 8, 128), F32),
+            pltpu.VMEM((OWN, 2048), BF16),
+            dma(()),
             pltpu.VMEM((2, SIZE, 2 * TOK), BF16),
             pltpu.VMEM((16, SLAB, 256), BF16),
             pltpu.VMEM((2, 8, 128), F32),
@@ -569,13 +654,13 @@
             pltpu.VMEM((4, OWN, 2048), BF16),
             pltpu.VMEM((3, OWN, 2048), BF16),
             pltpu.VMEM((3, OWN, 2048), BF16),
-            dma((32,)), dma((16,)), dma((16,)), dma((4,)), dma((2,)), dma((8,)), dma((8,)), dma((2,)), dma((4,)), dma((4,)),
+            dma((48,)), dma((16,)), dma((16,)), dma((16,)), dma((6,)), dma((3,)), dma((8,)), dma((8,)), dma((2,)), dma((4,)), dma((4,)),
             dma((3,)), dma((3,)),
         ],
         compiler_params=pltpu.CompilerParams(collective_id=0, has_side_effects=True, vmem_limit_bytes=63 << 20),
         cost_estimate=pl.CostEstimate(flops=4 * 768 * 12288 * 4 * 128, bytes_accessed=4 << 20, transcendentals=4 * 768 * 12288),
         name="attention",
-    )(q, kv, prm, w, up, down, residual, gains)
+    )(*operands)
 
 
 def layer_norm(activations, scales):
@@ -585,29 +670,10 @@
     return centred * lax.rsqrt(spread + EPSILON) * scales
 
 
-def kernel_operands(query_first, key_first, value_first, query_second, key_second, value_second, mix_lambda, head_gain):
-    first = query_first[:, 0].astype(F32) * (LOG2E / 8.0)
-    high = lax.reduce_precision(first, 8, 7)
-    low = first - high
-    second = query_second[:, 0].astype(F32) * (LOG2E / math.sqrt(128.0))
-    q = jnp.stack([
-        jnp.stack([jnp.concatenate([high[:, :64], low[:, :64]], 1), jnp.concatenate([high[:, 64:], low[:, 64:]], 1)]),
-        jnp.stack([second[:, :128], second[:, 128:]]),
-    ]).astype(BF16)
-    q = jnp.swapaxes(q, 2, 3)
-    one, two = key_first[:, 0, :64], key_first[:, 0, 64:]
-    keys = jnp.stack([jnp.concatenate([one, one, two, two], 1), key_second[:, 0]])
-    values = jnp.stack([value_first[:, 0], value_second[:, 0]])
-    values = jnp.swapaxes(values.reshape(2, 3, 256, VALUE), 2, 3).reshape(2, 3 * VALUE, 256)
-    kv = jnp.concatenate([keys, values], axis=1)
-    prm = jnp.concatenate([head_gain, jnp.broadcast_to(mix_lambda[:, :, None], (2, 1, 128)), jnp.zeros((2, 6, 128), F32)], axis=1)
-    return q, kv, prm
-
-
 def local(query_first, key_first, value_first, query_second, key_second, value_second, mix_lambda, head_gain, out_weight,
           residual, norm_gain, up_weight, down_weight):
-    q, kv, prm = kernel_operands(query_first, key_first, value_first, query_second, key_second, value_second, mix_lambda, head_gain)
-    return attention(q, kv, prm, out_weight.reshape(2 * VALUE, -1), up_weight, down_weight, residual, norm_gain)
+    return layer(query_first[:, 0], key_first[:, 0], value_first[:, 0], query_second[:, 0], key_second[:, 0], value_second[:, 0],
+                 mix_lambda, head_gain[:, 0], out_weight.reshape(2 * VALUE, -1), up_weight, down_weight, residual, norm_gain)
 
 
 def solution(mesh):

time: 165 us -> 144 us (0.87)
  Pallas kernels: 156 us -> 141 us
  other arithmetic: 3.32 us -> 0 us
  local copies, waits for them, and re-layouts: 5.02 us -> 3.07 us
    pallas_call x1, Pallas kernels: 156 us -> 141 us  [layer(): pl.pallas_call(attention_kernel, out_shape=jax.ShapeDtypeStruct((OWN, 204...]
    concatenate x2 -> x0, other arithmetic: 1.77 us -> none  [the longest x1 1.1 us: kernel_operands(): kv = jnp.concatenate([keys, values], axis=1)]
    unnamed x17 -> x4, local copies, waits for them, and re-layouts: 4.41 us -> 3.07 us
where the time goes in v3:
time: 144 us
  Pallas kernels  141 us (98%)
  local copies, waits for them, and re-layouts  3.07 us (2%)
    pallas_call x1, Pallas kernels, layer(): pl.pallas_call(attention_kernel, out_shape=jax.ShapeDtypeStruct((OWN, 204...  141 us
    unnamed x4, local copies, waits for them, and re-layouts  3.07 us

profile of v3, /device:TPU:1, one launch (start us, length us, event | category | flops | bytes accessed | tf_op | source)
XLA Modules:
  0.0 144.1 jit_solution(7047193952769740215)
XLA Ops:
  0.0 0.0 copy-start
  0.0 0.7 copy-done
  0.7 0.6 copy.14.mix_ref
  1.3 141.0 %attention.1 = bf16[96,2048]{1,0:T(8,128)(2,1)} custom-call(bf16[768,128]{1,0:T(8,128)(2,1)} %bitcast.11, bf16[768,128]{1,0:T(8,128)(2,1)} %bitcast.12, bf16[768,128]{1,0:T(8,128)(2,1)} %bitcast.13, bf16[768,256]{1,0:T(8,128)(2,1)} %bitcast.9, bf16[768,256]{1,0:T(8,128)(2,1)} %bitcast.10, bf16[768,128]{1,0:T(8,128)(2,1)} %bitcast.14, f32[2,1]{1,0:T(2,128)} %copy.14.mix_ref, ...), custom_call_target="tpu_custom_call" | custom-call | flops 19327352832 | bytes 4194304 | tf_op jit(solution)/shard_map/attention/pallas_call | solution.py:624
  142.4 1.8 %copy.16 = bf16[96,2048]{1,0:T(8,128)(2,1)} copy(bf16[96,2048]{1,0:T(8,128)(2,1)} %attention.1) | data formatting | bytes 786432
Async XLA Ops:
  0.0 0.7 copy-start

commit v4 on v3

--- a/solution.py
+++ b/solution.py
@@ -280,8 +280,8 @@
 
     kinds = (0, 0, 0, 0, 1, 2, 1, 1, 2, 2, 3, 1, 2, 3, 3, 3)
     order = (0, 1, 2, 3, 0, 0, 1, 2, 1, 2, 0, 3, 3, 1, 2, 3)
-    home_duties = {0: ((1, 0),), 1: ((0, 3),), 5: ((1, 1), (1, 2)), 8: ((1, 3),)}
-    away_duties = {1: ((2, 0),), 4: ((3, 0),), 5: ((2, 1), (2, 2)), 7: ((2, 3),), 9: ((3, 1), (3, 2)), 12: ((3, 3),)}
+    home_duties = {0: ((1, 0),), 1: ((0, 3),), 5: ((1, 1), (1, 2)), 10: ((1, 3),)}
+    away_duties = {1: ((2, 0),), 4: ((3, 0),), 5: ((2, 1), (2, 2)), 9: ((3, 1), (3, 2)), 10: ((2, 3),), 12: ((3, 3),)}
 
     def pick(i, table):
         value = jnp.int32(table[0])

time: 144 us -> 141 us (0.979)
  Pallas kernels: 141 us -> 138 us
    pallas_call x1, Pallas kernels: 141 us -> 138 us  [layer(): pl.pallas_call(attention_kernel, out_shape=jax.ShapeDtypeStruct((OWN, 204...]
where the time goes in v4:
time: 141 us
  Pallas kernels  138 us (98%)
  local copies, waits for them, and re-layouts  3.07 us (2%)
    pallas_call x1, Pallas kernels, layer(): pl.pallas_call(attention_kernel, out_shape=jax.ShapeDtypeStruct((OWN, 204...  138 us
    unnamed x4, local copies, waits for them, and re-layouts  3.07 us

profile of v4, /device:TPU:1, one launch (start us, length us, event | category | flops | bytes accessed | tf_op | source)
XLA Modules:
  0.0 140.6 jit_solution(6894331416441131090)
XLA Ops:
  0.0 0.0 copy-start
  0.0 0.7 copy-done
  0.7 0.6 copy.14.mix_ref
  1.3 137.6 %attention.1 = bf16[96,2048]{1,0:T(8,128)(2,1)} custom-call(bf16[768,128]{1,0:T(8,128)(2,1)} %bitcast.11, bf16[768,128]{1,0:T(8,128)(2,1)} %bitcast.12, bf16[768,128]{1,0:T(8,128)(2,1)} %bitcast.13, bf16[768,256]{1,0:T(8,128)(2,1)} %bitcast.9, bf16[768,256]{1,0:T(8,128)(2,1)} %bitcast.10, bf16[768,128]{1,0:T(8,128)(2,1)} %bitcast.14, f32[2,1]{1,0:T(2,128)} %copy.14.mix_ref, ...), custom_call_target="tpu_custom_call" | custom-call | flops 19327352832 | bytes 4194304 | tf_op jit(solution)/shard_map/attention/pallas_call | solution.py:624
  138.9 1.8 %copy.16 = bf16[96,2048]{1,0:T(8,128)(2,1)} copy(bf16[96,2048]{1,0:T(8,128)(2,1)} %attention.1) | data formatting | bytes 786432
Async XLA Ops:
  0.0 0.7 copy-start

commit v5 on v4

--- a/solution.py
+++ b/solution.py
@@ -281,7 +281,7 @@
     kinds = (0, 0, 0, 0, 1, 2, 1, 1, 2, 2, 3, 1, 2, 3, 3, 3)
     order = (0, 1, 2, 3, 0, 0, 1, 2, 1, 2, 0, 3, 3, 1, 2, 3)
     home_duties = {0: ((1, 0),), 1: ((0, 3),), 5: ((1, 1), (1, 2)), 10: ((1, 3),)}
-    away_duties = {1: ((2, 0),), 4: ((3, 0),), 5: ((2, 1), (2, 2)), 9: ((3, 1), (3, 2)), 10: ((2, 3),), 12: ((3, 3),)}
+    away_duties = {1: ((2, 0),), 4: ((3, 0),), 5: ((2, 1), (2, 2)), 9: ((3, 1), (3, 2)), 10: ((2, 3),), 13: ((3, 3),)}
 
     def pick(i, table):
         value = jnp.int32(table[0])

time: 141 us -> 139 us (0.986)
  Pallas kernels: 138 us -> 135 us
    pallas_call x1, Pallas kernels: 138 us -> 135 us  [layer(): pl.pallas_call(attention_kernel, out_shape=jax.ShapeDtypeStruct((OWN, 204...]
where the time goes in v5:
time: 139 us; the launch traced here: 138 us
  Pallas kernels  135 us (97%)
  local copies, waits for them, and re-layouts  3.07 us (2%)
    pallas_call x1, Pallas kernels, layer(): pl.pallas_call(attention_kernel, out_shape=jax.ShapeDtypeStruct((OWN, 204...  135 us
    unnamed x4, local copies, waits for them, and re-layouts  3.07 us

profile of v5, /device:TPU:1, one launch (start us, length us, event | category | flops | bytes accessed | tf_op | source)
XLA Modules:
  0.0 138.3 jit_solution(5979488863068251430)
XLA Ops:
  0.0 0.0 copy-start
  0.0 0.7 copy-done
  0.7 0.6 copy.14.mix_ref
  1.3 135.2 %attention.1 = bf16[96,2048]{1,0:T(8,128)(2,1)} custom-call(bf16[768,128]{1,0:T(8,128)(2,1)} %bitcast.11, bf16[768,128]{1,0:T(8,128)(2,1)} %bitcast.12, bf16[768,128]{1,0:T(8,128)(2,1)} %bitcast.13, bf16[768,256]{1,0:T(8,128)(2,1)} %bitcast.9, bf16[768,256]{1,0:T(8,128)(2,1)} %bitcast.10, bf16[768,128]{1,0:T(8,128)(2,1)} %bitcast.14, f32[2,1]{1,0:T(2,128)} %copy.14.mix_ref, ...), custom_call_target="tpu_custom_call" | custom-call | flops 19327352832 | bytes 4194304 | tf_op jit(solution)/shard_map/attention/pallas_call | solution.py:624
  136.5 1.8 %copy.16 = bf16[96,2048]{1,0:T(8,128)(2,1)} copy(bf16[96,2048]{1,0:T(8,128)(2,1)} %attention.1) | data formatting | bytes 786432
Async XLA Ops:
  0.0 0.7 copy-start

commit v6 on v5

--- a/solution.py
+++ b/solution.py
@@ -330,7 +330,7 @@
             columns(DOWN_A, False)
             columns(DOWN_A, True)
 
-        @pl.when(i == 6)
+        @pl.when(i == 7)
         def _():
             gathered(DOWN_B)
             columns(DOWN_B, False)
@@ -342,7 +342,7 @@
             columns(UP, False)
             columns(UP, True)
 
-        @pl.when(i == 10)
+        @pl.when(i == 11)
         def _():
             onward(DOWN_A)
             onward(DOWN_B)

time: 139 us -> 138 us (level)
  no operation moved by 1% of the time
where the time goes in v6:
time: 138 us; the launch traced here: 137 us
  Pallas kernels  134 us (97%)
  local copies, waits for them, and re-layouts  3.07 us (2%)
    pallas_call x1, Pallas kernels, layer(): pl.pallas_call(attention_kernel, out_shape=jax.ShapeDtypeStruct((OWN, 204...  134 us
    unnamed x4, local copies, waits for them, and re-layouts  3.07 us

profile of v6, /device:TPU:1, one launch (start us, length us, event | category | flops | bytes accessed | tf_op | source)
XLA Modules:
  0.0 137.2 jit_solution(12923245486374618551)
XLA Ops:
  0.0 0.0 copy-start
  0.0 0.7 copy-done
  0.7 0.6 copy.14.mix_ref
  1.3 134.2 %attention.1 = bf16[96,2048]{1,0:T(8,128)(2,1)} custom-call(bf16[768,128]{1,0:T(8,128)(2,1)} %bitcast.11, bf16[768,128]{1,0:T(8,128)(2,1)} %bitcast.12, bf16[768,128]{1,0:T(8,128)(2,1)} %bitcast.13, bf16[768,256]{1,0:T(8,128)(2,1)} %bitcast.9, bf16[768,256]{1,0:T(8,128)(2,1)} %bitcast.10, bf16[768,128]{1,0:T(8,128)(2,1)} %bitcast.14, f32[2,1]{1,0:T(2,128)} %copy.14.mix_ref, ...), custom_call_target="tpu_custom_call" | custom-call | flops 19327352832 | bytes 4194304 | tf_op jit(solution)/shard_map/attention/pallas_call | solution.py:624
  135.5 1.8 %copy.16 = bf16[96,2048]{1,0:T(8,128)(2,1)} copy(bf16[96,2048]{1,0:T(8,128)(2,1)} %attention.1) | data formatting | bytes 786432
Async XLA Ops:
  0.0 0.7 copy-start

commit v7 on v6

--- a/solution.py
+++ b/solution.py
@@ -342,7 +342,7 @@
             columns(UP, False)
             columns(UP, True)
 
-        @pl.when(i == 11)
+        @pl.when(i == 12)
         def _():
             onward(DOWN_A)
             onward(DOWN_B)

time: 138 us -> 138 us (level)
  no operation moved by 1% of the time
where the time goes in v7:
time: 138 us; the launch traced here: 136 us
  Pallas kernels  133 us (96%)
  local copies, waits for them, and re-layouts  3.07 us (2%)
    pallas_call x1, Pallas kernels, layer(): pl.pallas_call(attention_kernel, out_shape=jax.ShapeDtypeStruct((OWN, 204...  133 us
    unnamed x4, local copies, waits for them, and re-layouts  3.07 us

profile of v7, /device:TPU:1, one launch (start us, length us, event | category | flops | bytes accessed | tf_op | source)
XLA Modules:
  0.0 136.1 jit_solution(466972650156248410)
XLA Ops:
  0.0 0.0 copy-start
  0.0 0.7 copy-done
  0.7 0.6 copy.14.mix_ref
  1.3 133.1 %attention.1 = bf16[96,2048]{1,0:T(8,128)(2,1)} custom-call(bf16[768,128]{1,0:T(8,128)(2,1)} %bitcast.11, bf16[768,128]{1,0:T(8,128)(2,1)} %bitcast.12, bf16[768,128]{1,0:T(8,128)(2,1)} %bitcast.13, bf16[768,256]{1,0:T(8,128)(2,1)} %bitcast.9, bf16[768,256]{1,0:T(8,128)(2,1)} %bitcast.10, bf16[768,128]{1,0:T(8,128)(2,1)} %bitcast.14, f32[2,1]{1,0:T(2,128)} %copy.14.mix_ref, ...), custom_call_target="tpu_custom_call" | custom-call | flops 19327352832 | bytes 4194304 | tf_op jit(solution)/shard_map/attention/pallas_call | solution.py:624
  134.4 1.8 %copy.16 = bf16[96,2048]{1,0:T(8,128)(2,1)} copy(bf16[96,2048]{1,0:T(8,128)(2,1)} %attention.1) | data formatting | bytes 786432
Async XLA Ops:
  0.0 0.7 copy-start
